TPU v7x, 256 devices: a whole 4x4x8 slice. The times are simulated.
256 devices in a mesh: ep: 64 (over z, y, core), tp: 4 (over x).
Axes of the slice: x: 4, y: 4, z: 8, core: 2. Of those that a mesh axis runs over, the one named last changes fastest.
Arguments:
- mixer_in: bfloat16 [24576, 2048], P(('ep', 'tp')), may hold values from -8192 to 8192
- mixer_gain: float32 [2048], replicated, may hold values from 0.1 to 1.9
- query_weight: bfloat16 [2048, 512], P(None, 'tp'), may hold values from -4 to 4
- key_weight: bfloat16 [2048, 512], P(None, 'tp'), may hold values from -4 to 4
- value_weight: bfloat16 [2048, 512], P(None, 'tp'), may hold values from -0.125 to 0.125
- head_lambda: float32 [4], P('tp'), may hold values from 0.3 to 0.8
- head_gain: float32 [128], replicated, may hold values from 0.1 to 1.9
- out_weight: bfloat16 [512, 2048], P('tp'), may hold values from -0.25 to 0.25
- expert_in: bfloat16 [24576, 2048], P(('ep', 'tp')), may hold values from -6 to 6
- expert_gain: float32 [2048], replicated, may hold values from 0.1 to 1.9
- routes: int32 [24576, 2], P(('ep', 'tp')), may hold values from 0 to 63, all different within a row; in each aligned block of 96 rows (0 to 95, 96 to 191, ...) at most 6 rows name the same one
- route_weights: float32 [24576, 2], P(('ep', 'tp')), may hold values from 0.1 to 1
- gate_weight: bfloat16 [64, 2048, 512], P('ep'), may hold values from -0.125 to 0.125
- up_weight: bfloat16 [64, 2048, 512], P('ep'), may hold values from -0.125 to 0.125
- down_weight: bfloat16 [64, 512, 2048], P('ep'), may hold values from -0.25 to 0.25
- shared_gate: bfloat16 [2048, 512], P(None, 'tp'), may hold values from -0.125 to 0.125
- shared_up: bfloat16 [2048, 512], P(None, 'tp'), may hold values from -0.125 to 0.125
- shared_down: bfloat16 [512, 2048], P('tp'), may hold values from -0.25 to 0.25
Outputs:
- mixed_out: bfloat16 [24576, 2048], P(('ep', 'tp'))
- expert_out: bfloat16 [24576, 2048], P(('ep', 'tp'))
Inputs may be any that keep to these rules, and one draw needn't show every extreme that they name: `routes`: each row names 2 different experts. Among the 96 rows of one device no expert is named more than 6 times, and in every draw some device's rows name some expert exactly 6 times.
All inputs are finite; a program needn't handle non-finite values.
Results may differ from a plain program's by a relative error of at most 0.013.
The roundings to bfloat16 on the way count: a program that leaves them out, or rounds other values in their place, can miss the bound.
Values may be sent and summed in bfloat16 or wider, within the bound.
No kernel may reach another device: no remote copies, remote signals or barrier semaphores. Data moves between devices by JAX's collectives and lax.ppermute only.
A program may use at most 128 MiB of HBM per device.

v0:
```python
import functools

import jax
import jax.numpy as jnp
from jax import lax
from jax.experimental import pallas as pl
from jax.experimental.pallas import tpu as pltpu
from jax.sharding import Mesh
from jax.sharding import PartitionSpec as P


EP = ("ep_0", "ep_1", "ep_2")
EP_TP = ("ep_0", "ep_1", "ep_2", "tp")
EPS = 1e-06
ROUTED_SCALE = 2.5
LOG2E = 1.4426950408889634
BF = jnp.bfloat16
F32 = jnp.float32
VMEM = pl.BlockSpec(memory_space=pltpu.VMEM)
SMEM = pl.BlockSpec(memory_space=pltpu.SMEM)


def shift(x, axis, k):
    n = lax.axis_size(axis)
    return lax.ppermute(x, axis, [(i, (i + k) % n) for i in range(n)])


def call(kernel, ins, out_shape, flops, nbytes, trans=0, vmem=24, scratch=(), smem_out=()):
    single = not isinstance(out_shape, (list, tuple))
    outs = [out_shape] if single else list(out_shape)
    specs = [SMEM if i in smem_out else VMEM for i in range(len(outs))]
    return pl.pallas_call(
        kernel,
        out_shape=outs[0] if single else outs,
        in_specs=[spec for _, spec in ins],
        out_specs=specs[0] if single else specs,
        scratch_shapes=list(scratch),
        compiler_params=pltpu.CompilerParams(vmem_limit_bytes=vmem * 2**20),
        cost_estimate=pl.CostEstimate(flops=flops, bytes_accessed=nbytes, transcendentals=trans),
    )(*[a for a, _ in ins])


def ring4(x, axis, far):
    fwd = shift(x, axis, 1)
    bwd = shift(x, axis, -1)
    return x, fwd, bwd, shift(fwd if far > 0 else bwd, axis, far)


def rms_rows(matrix, scales):
    values_in = matrix.astype(F32)
    inverse = lax.rsqrt(jnp.mean(values_in * values_in, axis=-1, keepdims=True) + EPS)
    return values_in * inverse * scales


def project_kernel(r0, r1, r2, r3, wq, wk, wv, q_ref, kv_ref):
    rows = jnp.concatenate([r0[...], r1[...], r2[...], r3[...]], axis=0)
    width = wq.shape[1]
    q_ref[...] = jnp.dot(rows, wq[...], preferred_element_type=F32).astype(BF)
    kv_ref[:, :width] = jnp.dot(rows, wk[...], preferred_element_type=F32).astype(BF)
    kv_ref[:, width:] = jnp.dot(rows, wv[...], preferred_element_type=F32).astype(BF)


def silu_product(gate, up):
    return (gate / (1.0 + jnp.exp(-gate)) * up).astype(BF)


def shared_kernel(n, x0, x1, x2, x3, wg, wu, h0, h1, h2, h3):
    rows = jnp.concatenate([x[:n, :] for x in (x0, x1, x2, x3)], axis=0)
    gate = jnp.dot(rows, wg[...], preferred_element_type=F32)
    up = jnp.dot(rows, wu[...], preferred_element_type=F32)
    hidden = silu_product(gate, up)
    for i, h in enumerate((h0, h1, h2, h3)):
        h[...] = hidden[i * n : (i + 1) * n]


def to_tiles(tiles, rows):
    count, subs = rows.shape[0], rows.shape[1] // 128
    for j in range(subs):
        tiles[pl.ds(j, count, stride=subs), :] = rows[:, j * 128 : (j + 1) * 128]


def from_tiles(tiles, out):
    count, subs = out.shape[0], out.shape[1] // 128
    for j in range(subs):
        block = tiles[pl.ds(j, count, stride=subs), :]
        out[:, j * 128 : (j + 1) * 128] = block.astype(out.dtype)


def expert_kernel(x_ref, wg, wu, wd, out, tiles, rows):
    shape = x_ref.shape
    tiles[...] = x_ref[...].reshape(tiles.shape).astype(F32)
    from_tiles(tiles, rows)
    x = rows[...]
    gate = jnp.dot(x, wg[0], preferred_element_type=F32)
    up = jnp.dot(x, wu[0], preferred_element_type=F32)
    hidden = silu_product(gate, up)
    to_tiles(tiles, jnp.dot(hidden, wd[0], preferred_element_type=F32))
    out[...] = tiles[...].astype(BF).reshape(shape)


def split3(x):
    hi = x.astype(BF)
    rest = x - hi.astype(F32)
    mid = rest.astype(BF)
    low = (rest - mid.astype(F32)).astype(BF)
    return hi, mid, low


def store_lse(ref, index, rows, lse):
    hi, mid, low = split3(lse)
    packed = jnp.concatenate(
        [hi.astype(F32), mid.astype(F32), low.astype(F32), jnp.zeros_like(lse)], axis=0
    ).astype(BF)
    if index is None:
        ref[rows:, :] = packed
    else:
        ref[index, rows:, :] = packed


def load_lse(block):
    b = block.astype(F32)
    return b[0:8] + b[8:16] + b[16:24]


def attend_kernel(half, q0, q1, q2, q3, *refs):
    kvs, (own, peer), (k_ref, v_ref, q_all, o_all, s_ref, top_ref) = refs[:8], refs[8:10], refs[10:]
    width = k_ref.shape[1]
    at = 0
    for kv in kvs:
        n = kv.shape[0]
        k_ref[at : at + n, :] = kv[:, :width]
        v_ref[at : at + n, :] = kv[:, width:]
        at += n
    nq = q0.shape[0] // 2
    groups = nq // 128
    lane = lax.broadcasted_iota(jnp.int32, (1, width), 1)
    eye = lax.broadcasted_iota(jnp.int32, (128, 128), 0) == lax.broadcasted_iota(
        jnp.int32, (128, 128), 1
    )
    scale = half ** (-0.5)
    for y, q_ref in enumerate((q0, q1, q2, q3)):
        q_all[y] = q_ref[:nq, :]
        q_all[4 + y] = q_ref[nq:, :]

    def scores(y, c):
        q = q_all[y]
        qm = jnp.where((lane // half) == c, q, jnp.zeros_like(q))
        s = lax.dot_general(qm, k_ref[...], (((1,), (1,)), ((), ())), preferred_element_type=F32)
        s_ref[c] = s
        top_ref[c] = jnp.max(s, axis=1, keepdims=True)

    def read(y, c):
        top = top_ref[c]
        p = jnp.exp2((s_ref[c] - top) * (LOG2E * scale))
        total = jnp.sum(p, axis=1, keepdims=True)
        o = jnp.dot(p.astype(BF), v_ref[...], preferred_element_type=F32)
        o_all[y, c * nq : (c + 1) * nq, :] = (o / total).astype(BF)
        lse = top * scale + jnp.log(total)
        return [
            jnp.sum(jnp.where(eye, lse[g * 128 : (g + 1) * 128], 0.0), axis=0, keepdims=True)
            for g in range(groups)
        ]

    scores(0, 0)

    @pl.loop(0, 8)
    def _(y):
        scores(y, 1)
        rows = read(y, 0)
        scores(jnp.minimum(y + 1, 7), 0)
        rows += read(y, 1)
        rows += [jnp.zeros((1, 128), F32)] * (8 - len(rows))
        store_lse(o_all, y, 2 * nq, jnp.concatenate(rows, axis=0))

    own[...] = o_all[:4]
    peer[...] = o_all[4:]


def row_weights(w, g):
    return jnp.transpose(jnp.broadcast_to(w[g : g + 1, :], (128, 128)))


def merge_cores_kernel(own, rec, o0, o1, o2, o3):
    nrow = own.shape[1] - 32
    for y, out in enumerate((o0, o1, o2, o3)):
        la = load_lse(own[y, nrow:, :])
        lb = load_lse(rec[y, nrow:, :])
        top = jnp.maximum(la, lb)
        wa = jnp.exp(la - top)
        wb = jnp.exp(lb - top)
        total = wa + wb
        fa = wa / total
        fb = wb / total
        for g in range(nrow // 128):
            sl = slice(g * 128, (g + 1) * 128)
            out[sl, :] = (
                row_weights(fa, g) * own[y, sl, :].astype(F32)
                + row_weights(fb, g) * rec[y, sl, :].astype(F32)
            ).astype(BF)
        store_lse(out, None, nrow, top + jnp.log(total))


def merge_all_kernel(lam, p0, p1, p2, p3, gain, h0, h1, h2, h3, a0, a1, a2, a3, att):
    parts = (p0, p1, p2, p3)
    nrow = p0.shape[0] - 32
    lses = [load_lse(p[nrow:, :]) for p in parts]
    top = functools.reduce(jnp.maximum, lses)
    ws = [jnp.exp(x - top) for x in lses]
    total = functools.reduce(jnp.add, ws)
    fs = [w / total for w in ws]
    nq = nrow // 2
    lam0 = lam[0]
    for g in range(nq // 128):
        reads = []
        for c in range(2):
            at = c * nq + g * 128
            idx = at // 128
            acc = 0.0
            for f, p in zip(fs, parts):
                acc = acc + row_weights(f, idx) * p[at : at + 128, :].astype(F32)
            reads.append(acc)
        diff = reads[0] - lam0 * reads[1]
        inv = lax.rsqrt(jnp.mean(diff * diff, axis=1, keepdims=True) + EPS)
        att[g * 128 : (g + 1) * 128, :] = (diff * inv * gain[...] * (1.0 - lam0)).astype(BF)
    n = h0.shape[0]
    for i, (a, h) in enumerate(((a0, h0), (a1, h1), (a2, h2), (a3, h3))):
        a[:n, :] = att[i * n : (i + 1) * n, :]
        a[n:, :] = h[...]


def project_out_kernel(n, a0, a1, a2, a3, wo, wd, x1, x2, x3, routed, mixed, expert):
    depth = wo.shape[0]
    for i, (own, extra, out) in enumerate(((wo, None, mixed), (wd, routed, expert))):
        lo, hi = n + i * depth, n + (i + 1) * depth
        total = None if extra is None else extra[...]
        for a, w in zip((a0, a1, a2, a3), (own, x2, x1, x3)):
            rows = w[...] if w is own else w[lo:hi, :]
            part = jnp.dot(a[i * n : (i + 1) * n, :], rows, preferred_element_type=F32)
            part = part.astype(BF).astype(F32)
            total = part if total is None else total + part
        out[...] = total.astype(out.dtype)


def dispatch_kernel(capacity, top_count, x_ref, gain, routes, out, normed, slots, tiles, xf, count):
    x = x_ref[...].astype(F32)
    inverse = lax.rsqrt(jnp.mean(x * x, axis=1, keepdims=True) + EPS)
    x = x * inverse * gain[...]
    normed[...] = x.astype(BF)
    to_tiles(tiles, x)
    xf[...] = tiles[...].astype(BF).reshape(xf.shape)
    out[...] = jnp.zeros_like(out)
    for e in range(count.shape[0]):
        count[e] = 0

    def step(t, carry):
        row = xf[t]
        for k in range(top_count):
            i = t * top_count + k
            e = routes[i]
            c = count[e]
            count[e] = c + 1
            s = e * capacity + c
            slots[i] = s
            out[s] = row
        return carry

    lax.fori_loop(0, x_ref.shape[0], step, 0)


def combine_kernel(top_count, ret, slots, shares, out, tiles):
    subs = ret.shape[1]

    def step(t, carry):
        acc = None
        for k in range(top_count):
            i = t * top_count + k
            v = ret[slots[i]].astype(F32) * shares[i]
            acc = v if acc is None else acc + v
        tiles[pl.ds(pl.multiple_of(t * subs, subs), subs), :] = acc
        return carry

    lax.fori_loop(0, out.shape[0], step, 0)
    from_tiles(tiles, out)


def on_device(
    mixer_in,
    mixer_gain,
    query_weight,
    key_weight,
    value_weight,
    head_lambda,
    head_gain,
    out_weight,
    expert_in,
    expert_gain,
    routes,
    route_weights,
    gate_weight,
    up_weight,
    down_weight,
    shared_gate,
    shared_up,
    shared_down,
):
    tokens, width = mixer_in.shape
    vdim = head_gain.shape[0]
    half = query_weight.shape[1] // 2
    nq = 4 * tokens
    experts = lax.axis_size(EP)
    top_count = routes.shape[1]
    capacity = 2 * tokens * top_count // experts
    slots_all = experts * capacity
    lanes = 128
    subs = width // lanes
    S = jax.ShapeDtypeStruct

    normed_mixer = rms_rows(mixer_in, mixer_gain).astype(BF)
    shares = ROUTED_SCALE * route_weights / jnp.sum(route_weights, axis=1, keepdims=True)
    normed_mixer, shares = lax.optimization_barrier((normed_mixer, shares.reshape(-1)))
    mixer_rows = ring4(normed_mixer, "tp", 1)
    queries, kv = call(
        project_kernel,
        [(r, VMEM) for r in mixer_rows]
        + [(query_weight, VMEM), (key_weight, VMEM), (value_weight, VMEM)],
        [S((nq, 2 * half), BF), S((nq, 2 * half + vdim), BF)],
        flops=2 * nq * width * (4 * half + vdim),
        nbytes=4 * 10**6,
        vmem=12,
    )

    flat_routes = routes.reshape(-1)
    outgoing, normed_expert, slot_index = call(
        functools.partial(dispatch_kernel, capacity, top_count),
        [
            (expert_in, VMEM),
            (expert_gain.reshape(1, width), VMEM),
            (flat_routes, SMEM),
        ],
        [
            S((slots_all, subs, lanes), BF),
            S((tokens, width), BF),
            S((tokens * top_count,), jnp.int32),
        ],
        flops=10**7,
        nbytes=2 * 10**6,
        scratch=[
            pltpu.VMEM((tokens * subs, lanes), F32),
            pltpu.VMEM((tokens, subs, lanes), BF),
            pltpu.SMEM((experts,), jnp.int32),
        ],
        smem_out=(2,),
        vmem=12,
    )
    arrived = lax.all_to_all(
        outgoing.reshape(experts, capacity * subs, lanes), EP, 0, 0, tiled=True
    )

    kvs = [kv]
    fwd = bwd = kv
    for _ in range(3):
        fwd = shift(fwd, "ep_0", 1)
        bwd = shift(bwd, "ep_0", -1)
        kvs += [fwd, bwd]
    kvs += [shift(fwd, "ep_0", 1)]
    q_pair = jnp.concatenate([queries, shift(queries, "ep_2", 1)], axis=0)
    q_all = [q_pair] + [shift(q_pair, "ep_1", k) for k in (1, -1, 2)]

    normed_expert, _ = lax.optimization_barrier((normed_expert, mixer_rows[3]))
    joined = jnp.concatenate([normed_expert, out_weight, shared_down], axis=0)
    tails = ring4(joined, "tp", -1)
    hidden = call(
        functools.partial(shared_kernel, tokens),
        [(r, VMEM) for r in tails] + [(shared_gate, VMEM), (shared_up, VMEM)],
        [S((tokens, vdim), BF)] * 4,
        flops=4 * nq * width * vdim,
        nbytes=3 * 10**6,
        vmem=12,
    )

    result = call(
        expert_kernel,
        [
            (arrived.reshape(slots_all, subs, lanes), VMEM),
            (gate_weight, VMEM),
            (up_weight, VMEM),
            (down_weight, VMEM),
        ],
        S((slots_all, subs, lanes), BF),
        flops=6 * slots_all * width * gate_weight.shape[2],
        nbytes=10 * 10**6,
        scratch=[pltpu.VMEM((slots_all * subs, lanes), F32), pltpu.VMEM((slots_all, width), BF)],
        vmem=20,
    )
    returned = lax.all_to_all(result.reshape(experts, capacity * subs, lanes), EP, 0, 0, tiled=True)

    message = S((4, 2 * nq + 32, vdim), BF)
    keys = 8 * nq
    own, peer = call(
        functools.partial(attend_kernel, half),
        [(q, VMEM) for q in q_all] + [(b, VMEM) for b in kvs],
        [message, message],
        flops=2 * 2 * 8 * nq * keys * (2 * half + vdim),
        nbytes=6 * 10**6,
        trans=2 * 8 * nq * keys,
        vmem=32,
        scratch=[
            pltpu.VMEM((keys, 2 * half), BF),
            pltpu.VMEM((keys, vdim), BF),
            pltpu.VMEM((8, nq, 2 * half), BF),
            pltpu.VMEM((8, 2 * nq + 32, vdim), BF),
            pltpu.VMEM((2, nq, keys), F32),
            pltpu.VMEM((2, nq, 1), F32),
        ],
    )
    merged = call(
        merge_cores_kernel,
        [(own, VMEM), (shift(peer, "ep_2", 1), VMEM)],
        [S((2 * nq + 32, vdim), BF)] * 4,
        flops=5 * 10**7,
        nbytes=3 * 10**6,
        vmem=8,
    )
    parts = [merged[0]]
    for i, k in enumerate((-1, 1, 2)):
        parts.append(shift(merged[i + 1], "ep_1", k))
    attended = call(
        merge_all_kernel,
        [(head_lambda, SMEM)]
        + [(p, VMEM) for p in parts]
        + [(head_gain.reshape(1, vdim), VMEM)]
        + [(h, VMEM) for h in hidden],
        [S((2 * tokens, vdim), BF)] * 4,
        flops=5 * 10**7,
        nbytes=10**6,
        scratch=[pltpu.VMEM((nq, vdim), BF)],
        vmem=8,
    )
    backs = [attended[0]]
    for i, k in enumerate((-1, 1, 2)):
        backs.append(shift(attended[i + 1], "tp", k))
    routed = call(
        functools.partial(combine_kernel, top_count),
        [
            (returned.reshape(slots_all, subs, lanes), VMEM),
            (slot_index, SMEM),
            (shares, SMEM),
        ],
        S((tokens, width), F32),
        flops=10**7,
        nbytes=3 * 10**6,
        scratch=[pltpu.VMEM((tokens * subs, lanes), F32)],
        vmem=8,
    )
    mixed_out, expert_out = call(
        functools.partial(project_out_kernel, tokens),
        [(a, VMEM) for a in backs]
        + [(out_weight, VMEM), (shared_down, VMEM)]
        + [(w, VMEM) for w in tails[1:]]
        + [(routed, VMEM)],
        [S((tokens, width), BF), S((tokens, width), BF)],
        flops=16 * tokens * vdim * width,
        nbytes=8 * 10**6,
        vmem=12,
    )

    return (mixed_out, expert_out)


def solution(mesh):
    split = Mesh(mesh.devices.reshape(8, 4, 2, mesh.shape["tp"]), ("ep_0", "ep_1", "ep_2", "tp"))
    placed = (
        P(EP_TP, None),
        P(),
        P(None, "tp"),
        P(None, "tp"),
        P(None, "tp"),
        P("tp"),
        P(),
        P("tp", None),
        P(EP_TP, None),
        P(),
        P(EP_TP, None),
        P(EP_TP, None),
        P(EP, None, None),
        P(EP, None, None),
        P(EP, None, None),
        P(None, "tp"),
        P(None, "tp"),
        P("tp", None),
    )
    return jax.shard_map(
        on_device,
        mesh=split,
        in_specs=placed,
        out_specs=(P(EP_TP, None), P(EP_TP, None)),
        check_vma=False,
    )
```

profile of v0, /device:TPU:22, one launch (start us, length us, event | category | flops | bytes accessed | tf_op | source)
XLA Modules:
  0.0 198.3 jit_solution(1378584697336154627)
XLA Ops:
  3.2 3.7 %shard_map.188 = (bf16[384,16,128]{2,1,0:T(8,128)(2,1)}, bf16[96,2048]{1,0:T(8,128)(2,1)S(1)}, s32[192]{0:T(256)S(1)}) custom-call(bf16[96,2048]{1,0:T(8,128)(2,1)S(1)} %copy-done.19, f32[1,2048]{1,0:T(1,128)S(1)} %bitcast.8, s32[192]{0:T(256)S(1)} %reshape.41.routes), custom_call_target="tpu_custom_call" | custom-call | flops 10000000 | bytes 2000000 | tf_op jit(solution)/shard_map/pallas_call | solution.py:32
  7.7 12.1 %all-to-all-start = ((bf16[64,96,128]{2,1,0:T(8,128)(2,1)}), bf16[64,96,128]{2,1,0:T(8,128)(2,1)S(1)}, u32[]{:S(2)}, u32[]{:S(2)}) async-start(bf16[64,96,128]{2,1,0:T(8,128)(2,1)} %bitcast.2), calls=%async_computation | async-start | bytes 3145728 | tf_op jit(solution)/shard_map/all_to_all | solution.py:355
  21.7 10.9 %collective-permute-done.r1 = bf16[96,2048]{1,0:T(8,128)(2,1)S(1)} collective-permute-done((bf16[96,2048]{1,0:T(8,128)(2,1)}, bf16[96,2048]{1,0:T(8,128)(2,1)S(1)}, u32[]{:S(2)}, u32[]{:S(2)}) %collective-permute-start) | collective-permute-done | bytes 393248 | tf_op jit(solution)/shard_map/ppermute | solution.py:25
  34.3 8.6 %collective-permute-done.2.r3 = bf16[96,2048]{1,0:T(8,128)(2,1)S(1)} collective-permute-done((bf16[96,2048]{1,0:T(8,128)(2,1)S(1)}, bf16[96,2048]{1,0:T(8,128)(2,1)S(1)}, u32[]{:S(2)}, u32[]{:S(2)}) %collective-permute-start.2) | collective-permute-done | bytes 393248 | tf_op jit(solution)/shard_map/ppermute | solution.py:25
  42.9 1.9 constant_dynamic-update-slice_fusion.4
  47.9 12.0 %all-to-all-done = bf16[64,96,128]{2,1,0:T(8,128)(2,1)S(1)} async-done(((bf16[64,96,128]{2,1,0:T(8,128)(2,1)}), bf16[64,96,128]{2,1,0:T(8,128)(2,1)S(1)}, u32[]{:S(2)}, u32[]{:S(2)}) %all-to-all-start) | async-done | bytes 1572896 | tf_op jit(solution)/shard_map/all_to_all | solution.py:355
  64.6 5.3 %shard_map.191 = bf16[384,16,128]{2,1,0:T(8,128)(2,1)} custom-call(bf16[384,16,128]{2,1,0:T(8,128)(2,1)S(1)} %bitcast.6, bf16[1,2048,512]{2,1,0:T(8,128)(2,1)S(1)} %copy-done.7, bf16[1,2048,512]{2,1,0:T(8,128)(2,1)S(1)} %copy-done.8, bf16[1,512,2048]{2,1,0:T(8,128)(2,1)S(1)} %copy-done.9), custom_call_target="tpu_custom_call" | custom-call | flops 2415919104 | bytes 10000000 | tf_op jit(solution)/shard_map/pallas_call | solution.py:32
  70.0 5.4 %all-to-all-start.1 = ((bf16[64,96,128]{2,1,0:T(8,128)(2,1)}), bf16[64,96,128]{2,1,0:T(8,128)(2,1)S(1)}, u32[]{:S(2)}, u32[]{:S(2)}) async-start(bf16[64,96,128]{2,1,0:T(8,128)(2,1)} %bitcast.4), calls=%async_computation.1 | async-start | bytes 3145728 | tf_op jit(solution)/shard_map/all_to_all | solution.py:395
  75.4 13.0 %collective-permute-done.1.r2 = bf16[96,2048]{1,0:T(8,128)(2,1)} collective-permute-done((bf16[96,2048]{1,0:T(8,128)(2,1)}, bf16[96,2048]{1,0:T(8,128)(2,1)}, u32[]{:S(2)}, u32[]{:S(2)}) %collective-permute-start.1) | collective-permute-done | bytes 393248 | tf_op jit(solution)/shard_map/ppermute | solution.py:25
  93.5 2.5 %shard_map.185 = (bf16[384,128]{1,0:T(8,128)(2,1)S(1)}, bf16[384,256]{1,0:T(8,128)(2,1)S(1)}) custom-call(bf16[96,2048]{1,0:T(8,128)(2,1)} %fusion.2.r0, bf16[96,2048]{1,0:T(8,128)(2,1)S(1)} %copy-done.16, bf16[96,2048]{1,0:T(8,128)(2,1)} %collective-permute-done.1.r2, bf16[96,2048]{1,0:T(8,128)(2,1)S(1)} %copy-done.18, bf16[2048,128]{1,0:T(8,128)(2,1)S(1)} %copy-done.10, ...), custom_call_target="tpu_custom_call" | custom-call | flops 603979776 | bytes 4000000 | tf_op jit(solution)/shard_map/pallas_call | solution.py:32
  97.5 1.8 collective-permute-start.8
  99.3 17.7 %collective-permute-done.7.refs_1_ = bf16[384,256]{1,0:T(8,128)(2,1)S(1)} collective-permute-done((bf16[384,256]{1,0:T(8,128)(2,1)S(1)}, bf16[384,256]{1,0:T(8,128)(2,1)S(1)}, u32[]{:S(2)}, u32[]{:S(2)}) %collective-permute-start.7) | collective-permute-done | bytes 196640 | tf_op jit(solution)/shard_map/ppermute | solution.py:25
  117.7 3.2 %collective-permute-start.10 = (bf16[384,256]{1,0:T(8,128)(2,1)S(1)}, bf16[384,256]{1,0:T(8,128)(2,1)S(1)}, u32[]{:S(2)}, u32[]{:S(2)}) collective-permute-start(bf16[384,256]{1,0:T(8,128)(2,1)S(1)} %collective-permute-done.8.refs_2_), channel_id=1, source_target_pairs={{0,224},{32,0},{64,32},{96,64},{128,96},{160,128},{192,160},{224,1... | collective-permute-start | bytes 589832 | tf_op jit(solution)/shard_map/ppermute | solution.py:25
  121.0 3.7 %collective-permute-done.9.refs_3_ = bf16[384,256]{1,0:T(8,128)(2,1)S(1)} collective-permute-done((bf16[384,256]{1,0:T(8,128)(2,1)S(1)}, bf16[384,256]{1,0:T(8,128)(2,1)S(1)}, u32[]{:S(2)}, u32[]{:S(2)}) %collective-permute-start.9) | collective-permute-done | bytes 196640 | tf_op jit(solution)/shard_map/ppermute | solution.py:25
  126.7 3.2 %collective-permute-start.12 = (bf16[384,256]{1,0:T(8,128)(2,1)S(1)}, bf16[384,256]{1,0:T(8,128)(2,1)S(1)}, u32[]{:S(2)}, u32[]{:S(2)}) collective-permute-start(bf16[384,256]{1,0:T(8,128)(2,1)S(1)} %collective-permute-done.10.refs_4_), channel_id=1, source_target_pairs={{0,224},{32,0},{64,32},{96,64},{128,96},{160,128},{192,160},{224,1... | collective-permute-start | bytes 589832 | tf_op jit(solution)/shard_map/ppermute | solution.py:25
  133.6 4.8 %collective-permute-done.13.refs_7_ = bf16[384,256]{1,0:T(8,128)(2,1)S(1)} collective-permute-done((bf16[384,256]{1,0:T(8,128)(2,1)S(1)}, bf16[384,256]{1,0:T(8,128)(2,1)S(1)}, u32[]{:S(2)}, u32[]{:S(2)}) %collective-permute-start.13) | collective-permute-done | bytes 196640 | tf_op jit(solution)/shard_map/ppermute | solution.py:25
  138.4 28.8 %shard_map.186 = (bf16[4,800,128]{2,1,0:T(8,128)(2,1)S(1)}, bf16[4,800,128]{2,1,0:T(8,128)(2,1)S(1)}) custom-call(bf16[768,128]{1,0:T(8,128)(2,1)S(1)} %constant_dynamic-update-slice_fusion.q0, bf16[768,128]{1,0:T(8,128)(2,1)S(1)} %collective-permute-done.4.q1, bf16[768,128]{1,0:T(8,128)(2,1)S(1)} %collective-permute-done.5.q2, ...), custom_call_target="tpu_custom_call" | custom-call | flops 9663676416 | bytes 6000000 | tf_op jit(solution)/shard_map/pallas_call | solution.py:32
  167.3 2.3 %collective-permute-done.14.rec = bf16[4,800,128]{2,1,0:T(8,128)(2,1)S(1)} collective-permute-done((bf16[4,800,128]{2,1,0:T(8,128)(2,1)S(1)}, bf16[4,800,128]{2,1,0:T(8,128)(2,1)S(1)}, u32[]{:S(2)}, u32[]{:S(2)}) %collective-permute-start.14) | collective-permute-done | bytes 819232 | tf_op jit(solution)/shard_map/ppermute | solution.py:25
  174.6 3.4 %shard_map.189 = (bf16[96,128]{1,0:T(8,128)(2,1)S(1)}, bf16[96,128]{1,0:T(8,128)(2,1)S(1)}, bf16[96,128]{1,0:T(8,128)(2,1)S(1)}, bf16[96,128]{1,0:T(8,128)(2,1)S(1)}) custom-call(bf16[352,2048]{1,0:T(8,128)(2,1)} %constant_dynamic-update-slice_fusion.2.x0, bf16[352,2048]{1,0:T(8,128)(2,1)S(1)} %collective-permute-done.18.x1, ...), custom_call_target="tpu_custom_call" | custom-call | flops 402653184 | bytes 3000000 | tf_op jit(solution)/shard_map/pallas_call | solution.py:32
  178.5 4.8 %collective-permute-done.17.p3 = bf16[800,128]{1,0:T(8,128)(2,1)S(1)} collective-permute-done((bf16[800,128]{1,0:T(8,128)(2,1)S(1)}, bf16[800,128]{1,0:T(8,128)(2,1)S(1)}, u32[]{:S(2)}, u32[]{:S(2)}) %collective-permute-start.17) | collective-permute-done | bytes 204832 | tf_op jit(solution)/shard_map/ppermute | solution.py:25
  186.0 2.4 %collective-permute-start.22 = (bf16[192,128]{1,0:T(8,128)(2,1)}, bf16[192,128]{1,0:T(8,128)(2,1)}, u32[]{:S(2)}, u32[]{:S(2)}) collective-permute-start(bf16[192,128]{1,0:T(8,128)(2,1)} %get-tuple-element.41), channel_id=1, source_target_pairs={{0,1},{1,2},{2,3},{3,0},{4,5},{5,6},{6,7},{7,4},{8,9},{9,10},{10,1... | collective-permute-start | bytes 147464 | tf_op jit(solution)/shard_map/ppermute | solution.py:25
  188.6 1.8 shard_map.192.routed
  190.8 3.5 %collective-permute-done.23.a3 = bf16[192,128]{1,0:T(8,128)(2,1)} collective-permute-done((bf16[192,128]{1,0:T(8,128)(2,1)}, bf16[192,128]{1,0:T(8,128)(2,1)}, u32[]{:S(2)}, u32[]{:S(2)}) %collective-permute-start.23) | collective-permute-done | bytes 49184 | tf_op jit(solution)/shard_map/ppermute | solution.py:25
  195.7 2.6 %shard_map.193 = (bf16[96,2048]{1,0:T(8,128)(2,1)}, bf16[96,2048]{1,0:T(8,128)(2,1)}) custom-call(bf16[192,128]{1,0:T(8,128)(2,1)S(1)} %copy-done.22, bf16[192,128]{1,0:T(8,128)(2,1)} %collective-permute-done.21.a1, bf16[192,128]{1,0:T(8,128)(2,1)} %collective-permute-done.22.a2, bf16[192,128]{1,0:T(8,128)(2,1)} %collective-permute-done.23.a3, ...), custom_call_target="tpu_custom_call" | custom-call | flops 402653184 | bytes 8000000 | tf_op jit(solution)/shard_map/pallas_call | solution.py:32
  (107 shorter events, 37.3 us)
Async XLA Ops:
  7.7 52.1 %all-to-all-start = ((bf16[64,96,128]{2,1,0:T(8,128)(2,1)}), bf16[64,96,128]{2,1,0:T(8,128)(2,1)S(1)}, u32[]{:S(2)}, u32[]{:S(2)}) async-start(bf16[64,96,128]{2,1,0:T(8,128)(2,1)} %bitcast.2), calls=%async_computation | async-start | bytes 3145728 | tf_op jit(solution)/shard_map/all_to_all | solution.py:355
  21.2 11.3 %collective-permute-start = (bf16[96,2048]{1,0:T(8,128)(2,1)}, bf16[96,2048]{1,0:T(8,128)(2,1)S(1)}, u32[]{:S(2)}, u32[]{:S(2)}) collective-permute-start(bf16[96,2048]{1,0:T(8,128)(2,1)} %fusion.2.r0), channel_id=1, source_target_pairs={{0,1},{1,2},{2,3},{3,0},{4,5},{5,6},{6,7},{7,4},{8,9},{9,10},{10,1... | collective-permute-start | bytes 1179656 | tf_op jit(solution)/shard_map/ppermute | solution.py:25
  32.6 10.3 %collective-permute-start.2 = (bf16[96,2048]{1,0:T(8,128)(2,1)S(1)}, bf16[96,2048]{1,0:T(8,128)(2,1)S(1)}, u32[]{:S(2)}, u32[]{:S(2)}) collective-permute-start(bf16[96,2048]{1,0:T(8,128)(2,1)S(1)} %collective-permute-done.r1), channel_id=1, source_target_pairs={{0,1},{1,2},{2,3},{3,0},{4,5},{5,6},{6,7},{7,4},{8,9},{9,10},{10,1... | collective-permute-start | bytes 1179656 | tf_op jit(solution)/shard_map/ppermute | solution.py:25
  46.5 85.5 %collective-permute-start.19 = (bf16[352,2048]{1,0:T(8,128)(2,1)}, bf16[352,2048]{1,0:T(8,128)(2,1)S(1)}, u32[]{:S(2)}, u32[]{:S(2)}) collective-permute-start(bf16[352,2048]{1,0:T(8,128)(2,1)} %constant_dynamic-update-slice_fusion.2.x0), channel_id=1, source_target_pairs={{0,3},{1,0},{2,1},{3,2},{4,7},{5,4},{6,5},{7,6},{8,11},{9,8},{10,9... | collective-permute-start | bytes 4325384 | tf_op jit(solution)/shard_map/ppermute | solution.py:25
  47.3 41.0 %collective-permute-start.1 = (bf16[96,2048]{1,0:T(8,128)(2,1)}, bf16[96,2048]{1,0:T(8,128)(2,1)}, u32[]{:S(2)}, u32[]{:S(2)}) collective-permute-start(bf16[96,2048]{1,0:T(8,128)(2,1)} %fusion.2.r0), channel_id=1, source_target_pairs={{0,3},{1,0},{2,1},{3,2},{4,7},{5,4},{6,5},{7,6},{8,11},{9,8},{10,9... | collective-permute-start | bytes 1179656 | tf_op jit(solution)/shard_map/ppermute | solution.py:25
  70.0 118.7 %all-to-all-start.1 = ((bf16[64,96,128]{2,1,0:T(8,128)(2,1)}), bf16[64,96,128]{2,1,0:T(8,128)(2,1)S(1)}, u32[]{:S(2)}, u32[]{:S(2)}) async-start(bf16[64,96,128]{2,1,0:T(8,128)(2,1)} %bitcast.4), calls=%async_computation.1 | async-start | bytes 3145728 | tf_op jit(solution)/shard_map/all_to_all | solution.py:395
  96.0 21.1 %collective-permute-start.7 = (bf16[384,256]{1,0:T(8,128)(2,1)S(1)}, bf16[384,256]{1,0:T(8,128)(2,1)S(1)}, u32[]{:S(2)}, u32[]{:S(2)}) collective-permute-start(bf16[384,256]{1,0:T(8,128)(2,1)S(1)} %get-tuple-element.26.refs_0_), channel_id=1, source_target_pairs={{0,32},{32,64},{64,96},{96,128},{128,160},{160,192},{192,224},{224... | collective-permute-start | bytes 589832 | tf_op jit(solution)/shard_map/ppermute | solution.py:25
  97.5 20.2 %collective-permute-start.8 = (bf16[384,256]{1,0:T(8,128)(2,1)S(1)}, bf16[384,256]{1,0:T(8,128)(2,1)S(1)}, u32[]{:S(2)}, u32[]{:S(2)}) collective-permute-start(bf16[384,256]{1,0:T(8,128)(2,1)S(1)} %get-tuple-element.26.refs_0_), channel_id=1, source_target_pairs={{0,224},{32,0},{64,32},{96,64},{128,96},{160,128},{192,160},{224,1... | collective-permute-start | bytes 589832 | tf_op jit(solution)/shard_map/ppermute | solution.py:25
  99.3 17.8 %collective-permute-start.3 = (bf16[384,128]{1,0:T(8,128)(2,1)S(1)}, bf16[384,128]{1,0:T(8,128)(2,1)S(1)}, u32[]{:S(2)}, u32[]{:S(2)}) collective-permute-start(bf16[384,128]{1,0:T(8,128)(2,1)S(1)} %get-tuple-element.25), channel_id=1, source_target_pairs={{0,4},{4,0},{1,5},{5,1},{2,6},{6,2},{3,7},{7,3},{8,12},{12,8},{9,1... | collective-permute-start | bytes 294920 | tf_op jit(solution)/shard_map/ppermute | solution.py:25
  117.1 7.6 %collective-permute-start.9 = (bf16[384,256]{1,0:T(8,128)(2,1)S(1)}, bf16[384,256]{1,0:T(8,128)(2,1)S(1)}, u32[]{:S(2)}, u32[]{:S(2)}) collective-permute-start(bf16[384,256]{1,0:T(8,128)(2,1)S(1)} %collective-permute-done.7.refs_1_), channel_id=1, source_target_pairs={{0,32},{32,64},{64,96},{96,128},{128,160},{160,192},{192,224},{224... | collective-permute-start | bytes 589832 | tf_op jit(solution)/shard_map/ppermute | solution.py:25
  117.1 8.1 %collective-permute-start.6 = (bf16[768,128]{1,0:T(8,128)(2,1)S(1)}, bf16[768,128]{1,0:T(8,128)(2,1)S(1)}, u32[]{:S(2)}, u32[]{:S(2)}) collective-permute-start(bf16[768,128]{1,0:T(8,128)(2,1)S(1)} %constant_dynamic-update-slice_fusion.q0), channel_id=1, source_target_pairs={{0,16},{8,24},{16,0},{24,8},{1,17},{9,25},{17,1},{25,9},{2,18},{10... | collective-permute-start | bytes 589832 | tf_op jit(solution)/shard_map/ppermute | solution.py:25
  117.7 8.9 %collective-permute-start.10 = (bf16[384,256]{1,0:T(8,128)(2,1)S(1)}, bf16[384,256]{1,0:T(8,128)(2,1)S(1)}, u32[]{:S(2)}, u32[]{:S(2)}) collective-permute-start(bf16[384,256]{1,0:T(8,128)(2,1)S(1)} %collective-permute-done.8.refs_2_), channel_id=1, source_target_pairs={{0,224},{32,0},{64,32},{96,64},{128,96},{160,128},{192,160},{224,1... | collective-permute-start | bytes 589832 | tf_op jit(solution)/shard_map/ppermute | solution.py:25
  124.6 6.9 %collective-permute-start.11 = (bf16[384,256]{1,0:T(8,128)(2,1)S(1)}, bf16[384,256]{1,0:T(8,128)(2,1)S(1)}, u32[]{:S(2)}, u32[]{:S(2)}) collective-permute-start(bf16[384,256]{1,0:T(8,128)(2,1)S(1)} %collective-permute-done.9.refs_3_), channel_id=1, source_target_pairs={{0,32},{32,64},{64,96},{96,128},{128,160},{160,192},{192,224},{224... | collective-permute-start | bytes 589832 | tf_op jit(solution)/shard_map/ppermute | solution.py:25
  124.6 6.9 %collective-permute-start.5 = (bf16[768,128]{1,0:T(8,128)(2,1)S(1)}, bf16[768,128]{1,0:T(8,128)(2,1)S(1)}, u32[]{:S(2)}, u32[]{:S(2)}) collective-permute-start(bf16[768,128]{1,0:T(8,128)(2,1)S(1)} %constant_dynamic-update-slice_fusion.q0), channel_id=1, source_target_pairs={{0,24},{8,0},{16,8},{24,16},{1,25},{9,1},{17,9},{25,17},{2,26},{10... | collective-permute-start | bytes 589832 | tf_op jit(solution)/shard_map/ppermute | solution.py:25
  125.2 8.4 %collective-permute-start.4 = (bf16[768,128]{1,0:T(8,128)(2,1)S(1)}, bf16[768,128]{1,0:T(8,128)(2,1)S(1)}, u32[]{:S(2)}, u32[]{:S(2)}) collective-permute-start(bf16[768,128]{1,0:T(8,128)(2,1)S(1)} %constant_dynamic-update-slice_fusion.q0), channel_id=1, source_target_pairs={{0,8},{8,16},{16,24},{24,0},{1,9},{9,17},{17,25},{25,1},{2,10},{10... | collective-permute-start | bytes 589832 | tf_op jit(solution)/shard_map/ppermute | solution.py:25
  126.7 6.9 %collective-permute-start.12 = (bf16[384,256]{1,0:T(8,128)(2,1)S(1)}, bf16[384,256]{1,0:T(8,128)(2,1)S(1)}, u32[]{:S(2)}, u32[]{:S(2)}) collective-permute-start(bf16[384,256]{1,0:T(8,128)(2,1)S(1)} %collective-permute-done.10.refs_4_), channel_id=1, source_target_pairs={{0,224},{32,0},{64,32},{96,64},{128,96},{160,128},{192,160},{224,1... | collective-permute-start | bytes 589832 | tf_op jit(solution)/shard_map/ppermute | solution.py:25
  131.5 6.9 %collective-permute-start.13 = (bf16[384,256]{1,0:T(8,128)(2,1)S(1)}, bf16[384,256]{1,0:T(8,128)(2,1)S(1)}, u32[]{:S(2)}, u32[]{:S(2)}) collective-permute-start(bf16[384,256]{1,0:T(8,128)(2,1)S(1)} %collective-permute-done.11.refs_5_), channel_id=1, source_target_pairs={{0,32},{32,64},{64,96},{96,128},{128,160},{160,192},{192,224},{224... | collective-permute-start | bytes 589832 | tf_op jit(solution)/shard_map/ppermute | solution.py:25
  131.5 43.0 %collective-permute-start.18 = (bf16[352,2048]{1,0:T(8,128)(2,1)}, bf16[352,2048]{1,0:T(8,128)(2,1)S(1)}, u32[]{:S(2)}, u32[]{:S(2)}) collective-permute-start(bf16[352,2048]{1,0:T(8,128)(2,1)} %constant_dynamic-update-slice_fusion.2.x0), channel_id=1, source_target_pairs={{0,1},{1,2},{2,3},{3,0},{4,5},{5,6},{6,7},{7,4},{8,9},{9,10},{10,1... | collective-permute-start | bytes 4325384 | tf_op jit(solution)/shard_map/ppermute | solution.py:25
  132.0 42.5 %collective-permute-start.20 = (bf16[352,2048]{1,0:T(8,128)(2,1)S(1)}, bf16[352,2048]{1,0:T(8,128)(2,1)S(1)}, u32[]{:S(2)}, u32[]{:S(2)}) collective-permute-start(bf16[352,2048]{1,0:T(8,128)(2,1)S(1)} %collective-permute-done.19.x2), channel_id=1, source_target_pairs={{0,3},{1,0},{2,1},{3,2},{4,7},{5,4},{6,5},{7,6},{8,11},{9,8},{10,9... | collective-permute-start | bytes 4325384 | tf_op jit(solution)/shard_map/ppermute | solution.py:25
  170.5 8.0 %collective-permute-start.15 = (bf16[800,128]{1,0:T(8,128)(2,1)S(1)}, bf16[800,128]{1,0:T(8,128)(2,1)S(1)}, u32[]{:S(2)}, u32[]{:S(2)}) collective-permute-start(bf16[800,128]{1,0:T(8,128)(2,1)S(1)} %get-tuple-element.30), channel_id=1, source_target_pairs={{0,24},{8,0},{16,8},{24,16},{1,25},{9,1},{17,9},{25,17},{2,26},{10... | collective-permute-start | bytes 614408 | tf_op jit(solution)/shard_map/ppermute | solution.py:25
  171.1 7.4 %collective-permute-start.16 = (bf16[800,128]{1,0:T(8,128)(2,1)S(1)}, bf16[800,128]{1,0:T(8,128)(2,1)S(1)}, u32[]{:S(2)}, u32[]{:S(2)}) collective-permute-start(bf16[800,128]{1,0:T(8,128)(2,1)S(1)} %get-tuple-element.31), channel_id=1, source_target_pairs={{0,8},{8,16},{16,24},{24,0},{1,9},{9,17},{17,25},{25,1},{2,10},{10... | collective-permute-start | bytes 614408 | tf_op jit(solution)/shard_map/ppermute | solution.py:25
  172.6 10.7 %collective-permute-start.17 = (bf16[800,128]{1,0:T(8,128)(2,1)S(1)}, bf16[800,128]{1,0:T(8,128)(2,1)S(1)}, u32[]{:S(2)}, u32[]{:S(2)}) collective-permute-start(bf16[800,128]{1,0:T(8,128)(2,1)S(1)} %get-tuple-element.32), channel_id=1, source_target_pairs={{0,16},{8,24},{16,0},{24,8},{1,17},{9,25},{17,1},{25,9},{2,18},{10... | collective-permute-start | bytes 614408 | tf_op jit(solution)/shard_map/ppermute | solution.py:25
  185.2 5.6 %collective-permute-start.21 = (bf16[192,128]{1,0:T(8,128)(2,1)}, bf16[192,128]{1,0:T(8,128)(2,1)}, u32[]{:S(2)}, u32[]{:S(2)}) collective-permute-start(bf16[192,128]{1,0:T(8,128)(2,1)} %get-tuple-element.40), channel_id=1, source_target_pairs={{0,3},{1,0},{2,1},{3,2},{4,7},{5,4},{6,5},{7,6},{8,11},{9,8},{10,9... | collective-permute-start | bytes 147464 | tf_op jit(solution)/shard_map/ppermute | solution.py:25
  188.4 5.9 %collective-permute-start.23 = (bf16[192,128]{1,0:T(8,128)(2,1)}, bf16[192,128]{1,0:T(8,128)(2,1)}, u32[]{:S(2)}, u32[]{:S(2)}) collective-permute-start(bf16[192,128]{1,0:T(8,128)(2,1)} %get-tuple-element.42), channel_id=1, source_target_pairs={{0,2},{1,3},{2,0},{3,1},{4,6},{5,7},{6,4},{7,5},{8,10},{9,11},{10,... | collective-permute-start | bytes 147464 | tf_op jit(solution)/shard_map/ppermute | solution.py:25
  (30 other events, 172.6 us)
where the time goes:
time: 202 us; the launch traced here: 198 us
  waiting for transfers between devices  83.9 us (42%)
  Pallas kernels  50.2 us (25%)
  starting transfers between devices  42.4 us (21%)
  local copies, waits for them, and re-layouts  19.2 us (10%)
    ppermute x24, waiting for transfers between devices, shift(): return lax.ppermute(x, axis, [(i, (i + k) % n) for i in range(n)])  71.9 us
    pallas_call x9, Pallas kernels, call(): pl.pallas_call(kernel, out_shape=outs[0] if single else outs, in_specs=[s...  50.2 us
    ppermute x24, starting transfers between devices, shift(): return lax.ppermute(x, axis, [(i, (i + k) % n) for i in range(n)])  24.8 us
    unnamed x60, local copies, waits for them, and re-layouts  17.9 us
    all_to_all x1, starting transfers between devices, on_device(): lax.all_to_all(outgoing.reshape(experts, capacity * subs, lanes), EP, 0,...  12.1 us
    all_to_all x1, waiting for transfers between devices, on_device(): lax.all_to_all(outgoing.reshape(experts, capacity * subs, lanes), EP, 0,...  12 us
    all_to_all x1, starting transfers between devices, on_device(): lax.all_to_all(result.reshape(experts, capacity * subs, lanes), EP, 0, 0,...  5.42 us
  transfers between devices with their start and end apart: 26, of which 13 were waited for; matrix products, arithmetic and copies ran while one was open for 3% of the time, Pallas kernels for 22%

commit v1 on v0

--- a/solution.py
+++ b/solution.py
@@ -1,4 +1,5 @@
 import functools
+import math
 
 import jax
 import jax.numpy as jnp
@@ -18,6 +19,7 @@
 F32 = jnp.float32
 VMEM = pl.BlockSpec(memory_space=pltpu.VMEM)
 SMEM = pl.BlockSpec(memory_space=pltpu.SMEM)
+HBM = pl.BlockSpec(memory_space=pltpu.MemorySpace.HBM)
 
 
 def shift(x, axis, k):
@@ -40,10 +42,19 @@
     )(*[a for a, _ in ins])
 
 
-def ring4(x, axis, far):
+def forward_by_core(fwd, bwd, axis, k):
+    n = lax.axis_size(axis)
+    picked = jnp.where(lax.axis_index("ep_2") == 0, fwd, bwd)
+    last = axis == "tp"
+    place = (lambda c, i: c * n + i % n) if last else (lambda c, i: i % n * 2 + c)
+    pairs = [(place(c, i), place(c, i + d)) for c, d in ((0, k), (1, -k)) for i in range(n)]
+    return lax.ppermute(picked, ("ep_2", axis) if last else (axis, "ep_2"), pairs)
+
+
+def ring4(x, axis):
     fwd = shift(x, axis, 1)
     bwd = shift(x, axis, -1)
-    return x, fwd, bwd, shift(fwd if far > 0 else bwd, axis, far)
+    return x, fwd, bwd, forward_by_core(fwd, bwd, axis, 1)
 
 
 def rms_rows(matrix, scales):
@@ -64,13 +75,11 @@
     return (gate / (1.0 + jnp.exp(-gate)) * up).astype(BF)
 
 
-def shared_kernel(n, x0, x1, x2, x3, wg, wu, h0, h1, h2, h3):
+def shared_kernel(n, x0, x1, x2, x3, wg, wu, hidden):
     rows = jnp.concatenate([x[:n, :] for x in (x0, x1, x2, x3)], axis=0)
     gate = jnp.dot(rows, wg[...], preferred_element_type=F32)
     up = jnp.dot(rows, wu[...], preferred_element_type=F32)
-    hidden = silu_product(gate, up)
-    for i, h in enumerate((h0, h1, h2, h3)):
-        h[...] = hidden[i * n : (i + 1) * n]
+    hidden[...] = silu_product(gate, up)
 
 
 def to_tiles(tiles, rows):
@@ -86,15 +95,46 @@
         out[:, j * 128 : (j + 1) * 128] = block.astype(out.dtype)
 
 
-def expert_kernel(x_ref, wg, wu, wd, out, tiles, rows):
+def expert_kernel(x_ref, *refs):
+    weights, out, (tiles, rows, wg, wu, wd, hidden, sems) = refs[:3], refs[3], refs[4:]
+    step = 256
+    halves = hidden.shape[1] // step
+
+    def fetch(i, k):
+        cols = pl.ds(pl.multiple_of(i * step, step), step)
+        buf = (wg, wu)[k]
+        return pltpu.make_async_copy(weights[k].at[0, :, cols], buf.at[:, cols], sems.at[i, k])
+
+    last = pltpu.make_async_copy(weights[2].at[0], wd, sems.at[halves, 0])
+    for i in range(halves):
+        for k in range(2):
+            fetch(i, k).start()
+    last.start()
     shape = x_ref.shape
     tiles[...] = x_ref[...].reshape(tiles.shape).astype(F32)
     from_tiles(tiles, rows)
-    x = rows[...]
-    gate = jnp.dot(x, wg[0], preferred_element_type=F32)
-    up = jnp.dot(x, wu[0], preferred_element_type=F32)
-    hidden = silu_product(gate, up)
-    to_tiles(tiles, jnp.dot(hidden, wd[0], preferred_element_type=F32))
+
+    @pl.loop(0, halves)
+    def _(i):
+        fetch(i, 0).wait()
+        fetch(i, 1).wait()
+        cols = pl.ds(pl.multiple_of(i * step, step), step)
+        gate = jnp.dot(rows[...], wg[:, cols], preferred_element_type=F32)
+        up = jnp.dot(rows[...], wu[:, cols], preferred_element_type=F32)
+        hidden[:, cols] = silu_product(gate, up)
+
+    last.wait()
+    count, subs = rows.shape[0], rows.shape[1] // 128
+    wide = 512
+
+    @pl.loop(0, rows.shape[1] // wide)
+    def _(i):
+        cols = pl.ds(pl.multiple_of(i * wide, wide), wide)
+        part = jnp.dot(hidden[...], wd[:, cols], preferred_element_type=F32)
+        for j in range(wide // 128):
+            at = pl.ds(i * (wide // 128) + j, count, stride=subs)
+            tiles[at, :] = part[:, j * 128 : (j + 1) * 128]
+
     out[...] = tiles[...].astype(BF).reshape(shape)
 
 
@@ -106,15 +146,11 @@
     return hi, mid, low
 
 
-def store_lse(ref, index, rows, lse):
+def store_lse(ref, rows, lse):
     hi, mid, low = split3(lse)
-    packed = jnp.concatenate(
+    ref[rows:, :] = jnp.concatenate(
         [hi.astype(F32), mid.astype(F32), low.astype(F32), jnp.zeros_like(lse)], axis=0
     ).astype(BF)
-    if index is None:
-        ref[rows:, :] = packed
-    else:
-        ref[index, rows:, :] = packed
 
 
 def load_lse(block):
@@ -122,67 +158,106 @@
     return b[0:8] + b[8:16] + b[16:24]
 
 
-def attend_kernel(half, q0, q1, q2, q3, *refs):
-    kvs, (own, peer), (k_ref, v_ref, q_all, o_all, s_ref, top_ref) = refs[:8], refs[8:10], refs[10:]
-    width = k_ref.shape[1]
-    at = 0
-    for kv in kvs:
-        n = kv.shape[0]
-        k_ref[at : at + n, :] = kv[:, :width]
-        v_ref[at : at + n, :] = kv[:, width:]
-        at += n
-    nq = q0.shape[0] // 2
-    groups = nq // 128
+def attend_kernel(half, nq, picks, build, sizes, *refs):
+    qs = refs[: 1 + max(i for i, _ in picks)]
+    refs = refs[len(qs) :]
+    q_all, o_all, s_ref, top_ref, lse_ref = refs[-5:]
+    if build:
+        kvs, outs, (k_ref, v_ref) = refs[:8], refs[8:-7], refs[-7:-5]
+        width = k_ref.shape[1]
+        for i, kv in enumerate(kvs):
+            n = kv.shape[0]
+            k_ref[i * n : (i + 1) * n, :] = kv[:, :width]
+            v_ref[i * n : (i + 1) * n, :] = kv[:, width:]
+    else:
+        (k_ref, v_ref), outs = refs[:2], refs[2:-5]
+        width = k_ref.shape[1]
     lane = lax.broadcasted_iota(jnp.int32, (1, width), 1)
     eye = lax.broadcasted_iota(jnp.int32, (128, 128), 0) == lax.broadcasted_iota(
         jnp.int32, (128, 128), 1
     )
     scale = half ** (-0.5)
-    for y, q_ref in enumerate((q0, q1, q2, q3)):
-        q_all[y] = q_ref[:nq, :]
-        q_all[4 + y] = q_ref[nq:, :]
-
-    def scores(y, c):
-        q = q_all[y]
+    count = len(picks)
+    for y, (i, side) in enumerate(picks):
+        q_all[y * nq : (y + 1) * nq, :] = qs[i][side * nq : (side + 1) * nq, :]
+    size = s_ref.shape[1]
+    blocks, groups = count * nq // size, size // 128
+
+    def scores(b, c):
+        q = q_all[pl.ds(pl.multiple_of(b * size, size), size), :]
         qm = jnp.where((lane // half) == c, q, jnp.zeros_like(q))
         s = lax.dot_general(qm, k_ref[...], (((1,), (1,)), ((), ())), preferred_element_type=F32)
         s_ref[c] = s
         top_ref[c] = jnp.max(s, axis=1, keepdims=True)
 
-    def read(y, c):
+    def read(b, c):
         top = top_ref[c]
         p = jnp.exp2((s_ref[c] - top) * (LOG2E * scale))
         total = jnp.sum(p, axis=1, keepdims=True)
         o = jnp.dot(p.astype(BF), v_ref[...], preferred_element_type=F32)
-        o_all[y, c * nq : (c + 1) * nq, :] = (o / total).astype(BF)
+        o_all[c, pl.ds(pl.multiple_of(b * size, size), size), :] = (o / total).astype(BF)
         lse = top * scale + jnp.log(total)
-        return [
-            jnp.sum(jnp.where(eye, lse[g * 128 : (g + 1) * 128], 0.0), axis=0, keepdims=True)
-            for g in range(groups)
-        ]
+        for g in range(groups):
+            row = jnp.where(eye, lse[g * 128 : (g + 1) * 128], 0.0)
+            lse_ref[c, b, g : g + 1, :] = jnp.sum(row, axis=0, keepdims=True)
 
     scores(0, 0)
 
-    @pl.loop(0, 8)
-    def _(y):
-        scores(y, 1)
-        rows = read(y, 0)
-        scores(jnp.minimum(y + 1, 7), 0)
-        rows += read(y, 1)
-        rows += [jnp.zeros((1, 128), F32)] * (8 - len(rows))
-        store_lse(o_all, y, 2 * nq, jnp.concatenate(rows, axis=0))
-
-    own[...] = o_all[:4]
-    peer[...] = o_all[4:]
+    @pl.loop(0, blocks)
+    def _(b):
+        scores(b, 1)
+        read(b, 0)
+        scores(jnp.minimum(b + 1, blocks - 1), 0)
+        read(b, 1)
+
+    parts = nq // 128
+    y = 0
+    for out, number in zip(outs, sizes):
+        for k in range(number):
+            ref = out.at[k] if number > 1 else out
+            rows = []
+            for c in range(2):
+                ref[c * nq : (c + 1) * nq, :] = o_all[c, y * nq : (y + 1) * nq, :]
+                for g in range(y * parts, (y + 1) * parts):
+                    rows.append(lse_ref[c, g // groups, g % groups : g % groups + 1, :])
+            rows.append(jnp.zeros((8 - 2 * parts, 128), F32))
+            store_lse(ref, 2 * nq, jnp.concatenate(rows, axis=0))
+            y += 1
+
+
+def attend(half, nq, qs, keys_values, picks, groups):
+    build = len(keys_values) == 8
+    rows, count = 2 * nq + 32, len(picks)
+    keys, vdim, block = 8 * nq, 128, math.gcd(256, count * nq)
+    S = jax.ShapeDtypeStruct
+    outs = [S((n, rows, vdim) if n > 1 else (rows, vdim), BF) for n in groups]
+    if build:
+        outs += [S((keys, 2 * half), BF), S((keys, vdim), BF)]
+    return call(
+        functools.partial(attend_kernel, half, nq, picks, build, groups),
+        [(q, VMEM) for q in qs] + [(b, VMEM) for b in keys_values],
+        outs,
+        flops=4 * count * nq * keys * (2 * half + vdim),
+        nbytes=4 * 10**6,
+        trans=2 * count * nq * keys,
+        vmem=24,
+        scratch=[
+            pltpu.VMEM((count * nq, 2 * half), BF),
+            pltpu.VMEM((2, count * nq, vdim), BF),
+            pltpu.VMEM((2, block, keys), F32),
+            pltpu.VMEM((2, block, 1), F32),
+            pltpu.VMEM((2, count * nq // block, 8, 128), F32),
+        ],
+    )
 
 
 def row_weights(w, g):
     return jnp.transpose(jnp.broadcast_to(w[g : g + 1, :], (128, 128)))
 
 
-def merge_cores_kernel(own, rec, o0, o1, o2, o3):
+def merge_cores_kernel(own, rec, o0, o1, o2):
     nrow = own.shape[1] - 32
-    for y, out in enumerate((o0, o1, o2, o3)):
+    for y, out in enumerate((o0, o1, o2)):
         la = load_lse(own[y, nrow:, :])
         lb = load_lse(rec[y, nrow:, :])
         top = jnp.maximum(la, lb)
@@ -197,12 +272,12 @@
                 row_weights(fa, g) * own[y, sl, :].astype(F32)
                 + row_weights(fb, g) * rec[y, sl, :].astype(F32)
             ).astype(BF)
-        store_lse(out, None, nrow, top + jnp.log(total))
-
-
-def merge_all_kernel(lam, p0, p1, p2, p3, gain, h0, h1, h2, h3, a0, a1, a2, a3, att):
-    parts = (p0, p1, p2, p3)
-    nrow = p0.shape[0] - 32
+        store_lse(out, nrow, top + jnp.log(total))
+
+
+def merge_all_kernel(lam, own, rec, p1, p2, p3, gain, hidden, a0, a1, a2, a3, att):
+    parts = (own, rec, p1, p2, p3)
+    nrow = own.shape[0] - 32
     lses = [load_lse(p[nrow:, :]) for p in parts]
     top = functools.reduce(jnp.maximum, lses)
     ws = [jnp.exp(x - top) for x in lses]
@@ -222,10 +297,10 @@
         diff = reads[0] - lam0 * reads[1]
         inv = lax.rsqrt(jnp.mean(diff * diff, axis=1, keepdims=True) + EPS)
         att[g * 128 : (g + 1) * 128, :] = (diff * inv * gain[...] * (1.0 - lam0)).astype(BF)
-    n = h0.shape[0]
-    for i, (a, h) in enumerate(((a0, h0), (a1, h1), (a2, h2), (a3, h3))):
+    n = nq // 4
+    for i, a in enumerate((a0, a1, a2, a3)):
         a[:n, :] = att[i * n : (i + 1) * n, :]
-        a[n:, :] = h[...]
+        a[n:, :] = hidden[i * n : (i + 1) * n, :]
 
 
 def project_out_kernel(n, a0, a1, a2, a3, wo, wd, x1, x2, x3, routed, mixed, expert):
@@ -316,9 +391,7 @@
     S = jax.ShapeDtypeStruct
 
     normed_mixer = rms_rows(mixer_in, mixer_gain).astype(BF)
-    shares = ROUTED_SCALE * route_weights / jnp.sum(route_weights, axis=1, keepdims=True)
-    normed_mixer, shares = lax.optimization_barrier((normed_mixer, shares.reshape(-1)))
-    mixer_rows = ring4(normed_mixer, "tp", 1)
+    mixer_rows = ring4(normed_mixer, "tp")
     queries, kv = call(
         project_kernel,
         [(r, VMEM) for r in mixer_rows]
@@ -356,23 +429,23 @@
         outgoing.reshape(experts, capacity * subs, lanes), EP, 0, 0, tiled=True
     )
 
-    kvs = [kv]
-    fwd = bwd = kv
-    for _ in range(3):
-        fwd = shift(fwd, "ep_0", 1)
-        bwd = shift(bwd, "ep_0", -1)
-        kvs += [fwd, bwd]
-    kvs += [shift(fwd, "ep_0", 1)]
+    shares = ROUTED_SCALE * route_weights / jnp.sum(route_weights, axis=1, keepdims=True)
+    queries, shares = lax.optimization_barrier((queries, shares.reshape(-1)))
+
+    near = [shift(kv, "ep_0", k) for k in (1, -1, 2, -2)]
+    far = [shift(near[2], "ep_0", 1), shift(near[3], "ep_0", -1)]
+    far.append(shift(near[3], "ep_0", -2))
+    kvs = [kv] + near + far
     q_pair = jnp.concatenate([queries, shift(queries, "ep_2", 1)], axis=0)
     q_all = [q_pair] + [shift(q_pair, "ep_1", k) for k in (1, -1, 2)]
 
-    normed_expert, _ = lax.optimization_barrier((normed_expert, mixer_rows[3]))
+    normed_expert, _ = lax.optimization_barrier((normed_expert, mixer_rows[1]))
     joined = jnp.concatenate([normed_expert, out_weight, shared_down], axis=0)
-    tails = ring4(joined, "tp", -1)
+    tails = ring4(joined, "tp")
     hidden = call(
         functools.partial(shared_kernel, tokens),
         [(r, VMEM) for r in tails] + [(shared_gate, VMEM), (shared_up, VMEM)],
-        [S((tokens, vdim), BF)] * 4,
+        S((nq, vdim), BF),
         flops=4 * nq * width * vdim,
         nbytes=3 * 10**6,
         vmem=12,
@@ -382,54 +455,47 @@
         expert_kernel,
         [
             (arrived.reshape(slots_all, subs, lanes), VMEM),
-            (gate_weight, VMEM),
-            (up_weight, VMEM),
-            (down_weight, VMEM),
+            (gate_weight, HBM),
+            (up_weight, HBM),
+            (down_weight, HBM),
         ],
         S((slots_all, subs, lanes), BF),
         flops=6 * slots_all * width * gate_weight.shape[2],
         nbytes=10 * 10**6,
-        scratch=[pltpu.VMEM((slots_all * subs, lanes), F32), pltpu.VMEM((slots_all, width), BF)],
-        vmem=20,
+        scratch=[
+            pltpu.VMEM((slots_all * subs, lanes), F32),
+            pltpu.VMEM((slots_all, width), BF),
+            pltpu.VMEM(gate_weight.shape[1:], BF),
+            pltpu.VMEM(up_weight.shape[1:], BF),
+            pltpu.VMEM(down_weight.shape[1:], BF),
+            pltpu.VMEM((slots_all, gate_weight.shape[2]), BF),
+            pltpu.SemaphoreType.DMA((gate_weight.shape[2] // 256 + 1, 2)),
+        ],
+        vmem=54,
     )
     returned = lax.all_to_all(result.reshape(experts, capacity * subs, lanes), EP, 0, 0, tiled=True)
 
-    message = S((4, 2 * nq + 32, vdim), BF)
-    keys = 8 * nq
-    own, peer = call(
-        functools.partial(attend_kernel, half),
-        [(q, VMEM) for q in q_all] + [(b, VMEM) for b in kvs],
-        [message, message],
-        flops=2 * 2 * 8 * nq * keys * (2 * half + vdim),
-        nbytes=6 * 10**6,
-        trans=2 * 8 * nq * keys,
-        vmem=32,
-        scratch=[
-            pltpu.VMEM((keys, 2 * half), BF),
-            pltpu.VMEM((keys, vdim), BF),
-            pltpu.VMEM((8, nq, 2 * half), BF),
-            pltpu.VMEM((8, 2 * nq + 32, vdim), BF),
-            pltpu.VMEM((2, nq, keys), F32),
-            pltpu.VMEM((2, nq, 1), F32),
-        ],
-    )
+    sides = tuple((i, side) for side in (1, 0) for i in (1, 2, 3))
+    peer, own, keys_all, values_all = attend(half, nq, q_all, kvs, sides, (3, 3))
+    received = shift(peer, "ep_2", 1)
+    peer0, own0 = attend(half, nq, q_all[:1], [keys_all, values_all], ((0, 1), (0, 0)), (1, 1))
     merged = call(
         merge_cores_kernel,
-        [(own, VMEM), (shift(peer, "ep_2", 1), VMEM)],
-        [S((2 * nq + 32, vdim), BF)] * 4,
+        [(own, VMEM), (received, VMEM)],
+        [S((2 * nq + 32, vdim), BF)] * 3,
         flops=5 * 10**7,
         nbytes=3 * 10**6,
         vmem=8,
     )
-    parts = [merged[0]]
+    parts = [own0, shift(peer0, "ep_2", 1)]
     for i, k in enumerate((-1, 1, 2)):
-        parts.append(shift(merged[i + 1], "ep_1", k))
+        parts.append(shift(merged[i], "ep_1", k))
     attended = call(
         merge_all_kernel,
         [(head_lambda, SMEM)]
         + [(p, VMEM) for p in parts]
         + [(head_gain.reshape(1, vdim), VMEM)]
-        + [(h, VMEM) for h in hidden],
+        + [(hidden, VMEM)],
         [S((2 * tokens, vdim), BF)] * 4,
         flops=5 * 10**7,
         nbytes=10**6,

time: 202 us -> 205 us (1.015)
  the two profiles are of different devices: /device:TPU:22 before, /device:TPU:66 now
where the time goes in v1:
time: 205 us; the launch traced here: 204 us
  waiting for transfers between devices  79.7 us (39%)
  Pallas kernels  56.5 us (28%)
  starting transfers between devices  51.3 us (25%)
  local copies, waits for them, and re-layouts  12.1 us (6%)
  other arithmetic  3.07 us (1%)
    pallas_call x10, Pallas kernels, call(): pl.pallas_call(kernel, out_shape=outs[0] if single else outs, in_specs=[s...  56.5 us
    ppermute x23, waiting for transfers between devices, shift(): return lax.ppermute(x, axis, [(i, (i + k) % n) for i in range(n)])  51.6 us
    ppermute x23, starting transfers between devices, shift(): return lax.ppermute(x, axis, [(i, (i + k) % n) for i in range(n)])  30.6 us
    all_to_all x1, waiting for transfers between devices, on_device(): lax.all_to_all(outgoing.reshape(experts, capacity * subs, lanes), EP, 0,...  22.3 us
    all_to_all x1, starting transfers between devices, on_device(): lax.all_to_all(outgoing.reshape(experts, capacity * subs, lanes), EP, 0,...  11.5 us
    unnamed x46, local copies, waits for them, and re-layouts  10.4 us
    all_to_all x1, starting transfers between devices, on_device(): lax.all_to_all(result.reshape(experts, capacity * subs, lanes), EP, 0, 0,...  6.16 us
    ppermute x2, waiting for transfers between devices, forward_by_core(): lax.ppermute(picked, ('ep_2', axis) if last else (axis, 'ep_2'), pairs)  5.78 us
  transfers between devices with their start and end apart: 27, of which 11 were waited for; matrix products, arithmetic and copies ran while one was open for 3% of the time, Pallas kernels for 25%

profile of v1, /device:TPU:66, one launch (start us, length us, event | category | flops | bytes accessed | tf_op | source)
XLA Modules:
  0.0 204.3 jit_solution(2872674281329315521)
XLA Ops:
  3.2 3.7 %shard_map.189 = (bf16[384,16,128]{2,1,0:T(8,128)(2,1)}, bf16[96,2048]{1,0:T(8,128)(2,1)S(1)}, s32[192]{0:T(256)S(1)}) custom-call(bf16[96,2048]{1,0:T(8,128)(2,1)S(1)} %copy-done.12, f32[1,2048]{1,0:T(1,128)S(1)} %bitcast.6, s32[192]{0:T(256)S(1)} %reshape.41.routes), custom_call_target="tpu_custom_call" | custom-call | flops 10000000 | bytes 2000000 | tf_op jit(solution)/shard_map/pallas_call | solution.py:34
  7.5 11.5 %all-to-all-start = ((bf16[64,96,128]{2,1,0:T(8,128)(2,1)}), bf16[64,96,128]{2,1,0:T(8,128)(2,1)}, u32[]{:S(2)}, u32[]{:S(2)}) async-start(bf16[64,96,128]{2,1,0:T(8,128)(2,1)} %bitcast.2), calls=%async_computation | async-start | bytes 3145728 | tf_op jit(solution)/shard_map/all_to_all | solution.py:428
  22.1 9.3 %collective-permute-done.r1 = bf16[96,2048]{1,0:T(8,128)(2,1)S(1)} collective-permute-done((bf16[96,2048]{1,0:T(8,128)(2,1)}, bf16[96,2048]{1,0:T(8,128)(2,1)S(1)}, u32[]{:S(2)}, u32[]{:S(2)}) %collective-permute-start) | collective-permute-done | bytes 393248 | tf_op jit(solution)/shard_map/ppermute | solution.py:27
  36.1 22.3 %all-to-all-done = bf16[64,96,128]{2,1,0:T(8,128)(2,1)} async-done(((bf16[64,96,128]{2,1,0:T(8,128)(2,1)}), bf16[64,96,128]{2,1,0:T(8,128)(2,1)}, u32[]{:S(2)}, u32[]{:S(2)}) %all-to-all-start) | async-done | bytes 1572896 | tf_op jit(solution)/shard_map/all_to_all | solution.py:428
  58.3 8.5 %shard_map.192 = bf16[384,16,128]{2,1,0:T(8,128)(2,1)} custom-call(bf16[384,16,128]{2,1,0:T(8,128)(2,1)} %bitcast.3.x_ref, bf16[1,2048,512]{2,1,0:T(8,128)(2,1)} %refs_0_.1, bf16[1,2048,512]{2,1,0:T(8,128)(2,1)} %refs_1_.1, bf16[1,512,2048]{2,1,0:T(8,128)(2,1)} %refs_2_.1), custom_call_target="tpu_custom_call" | custom-call | flops 2415919104 | bytes 10000000 | tf_op jit(solution)/shard_map/pallas_call | solution.py:34
  66.9 6.2 %all-to-all-start.1 = ((bf16[64,96,128]{2,1,0:T(8,128)(2,1)}), bf16[64,96,128]{2,1,0:T(8,128)(2,1)}, u32[]{:S(2)}, u32[]{:S(2)}) async-start(bf16[64,96,128]{2,1,0:T(8,128)(2,1)} %bitcast.8), calls=%async_computation.1 | async-start | bytes 3145728 | tf_op jit(solution)/shard_map/all_to_all | solution.py:476
  73.0 1.8 broadcast_select_fusion.1
  77.2 5.8 %collective-permute-done.2.r3 = bf16[96,2048]{1,0:T(8,128)(2,1)} collective-permute-done((bf16[96,2048]{1,0:T(8,128)(2,1)}, bf16[96,2048]{1,0:T(8,128)(2,1)}, u32[]{:S(2)}, u32[]{:S(2)}) %collective-permute-start.2) | collective-permute-done | bytes 393248 | tf_op jit(solution)/shard_map/ppermute | solution.py:51
  87.1 2.6 %shard_map.185 = (bf16[384,128]{1,0:T(8,128)(2,1)S(1)}, bf16[384,256]{1,0:T(8,128)(2,1)S(1)}) custom-call(bf16[96,2048]{1,0:T(8,128)(2,1)} %fusion.2.r0, bf16[96,2048]{1,0:T(8,128)(2,1)S(1)} %copy-done.6, bf16[96,2048]{1,0:T(8,128)(2,1)} %collective-permute-done.1.r2, bf16[96,2048]{1,0:T(8,128)(2,1)} %collective-permute-done.2.r3, ...), custom_call_target="tpu_custom_call" | custom-call | flops 603979776 | bytes 4000000 | tf_op jit(solution)/shard_map/pallas_call | solution.py:34
  90.3 3.6 %collective-permute-start.9 = (bf16[384,256]{1,0:T(8,128)(2,1)S(1)}, bf16[384,256]{1,0:T(8,128)(2,1)S(1)}, u32[]{:S(2)}, u32[]{:S(2)}) collective-permute-start(bf16[384,256]{1,0:T(8,128)(2,1)S(1)} %get-tuple-element.25.refs_4_), channel_id=1, source_target_pairs={{0,64},{32,96},{64,128},{96,160},{128,192},{160,224},{192,0},{224,... | collective-permute-start | bytes 589832 | tf_op jit(solution)/shard_map/ppermute | solution.py:27
  95.2 24.4 %collective-permute-done.10.refs_8_ = bf16[384,256]{1,0:T(8,128)(2,1)S(1)} collective-permute-done((bf16[384,256]{1,0:T(8,128)(2,1)S(1)}, bf16[384,256]{1,0:T(8,128)(2,1)S(1)}, u32[]{:S(2)}, u32[]{:S(2)}) %collective-permute-start.10) | collective-permute-done | bytes 196640 | tf_op jit(solution)/shard_map/ppermute | solution.py:27
  120.3 3.0 %collective-permute-start.6 = (bf16[768,128]{1,0:T(8,128)(2,1)S(1)}, bf16[768,128]{1,0:T(8,128)(2,1)S(1)}, u32[]{:S(2)}, u32[]{:S(2)}) collective-permute-start(bf16[768,128]{1,0:T(8,128)(2,1)S(1)} %constant_dynamic-update-slice_fusion.refs_0_), channel_id=1, source_target_pairs={{0,16},{8,24},{16,0},{24,8},{1,17},{9,25},{17,1},{25,9},{2,18},{10... | collective-permute-start | bytes 589832 | tf_op jit(solution)/shard_map/ppermute | solution.py:27
  125.4 2.0 collective-permute-start.4
  128.0 2.6 %collective-permute-start.12 = (bf16[384,256]{1,0:T(8,128)(2,1)S(1)}, bf16[384,256]{1,0:T(8,128)(2,1)S(1)}, u32[]{:S(2)}, u32[]{:S(2)}) collective-permute-start(bf16[384,256]{1,0:T(8,128)(2,1)S(1)} %collective-permute-done.10.refs_8_), channel_id=1, source_target_pairs={{0,224},{32,0},{64,32},{96,64},{128,96},{160,128},{192,160},{224,1... | collective-permute-start | bytes 589832 | tf_op jit(solution)/shard_map/ppermute | solution.py:27
  133.4 7.4 %collective-permute-done.13.refs_11_ = bf16[384,256]{1,0:T(8,128)(2,1)S(1)} collective-permute-done((bf16[384,256]{1,0:T(8,128)(2,1)S(1)}, bf16[384,256]{1,0:T(8,128)(2,1)S(1)}, u32[]{:S(2)}, u32[]{:S(2)}) %collective-permute-start.13) | collective-permute-done | bytes 196640 | tf_op jit(solution)/shard_map/ppermute | solution.py:27
  141.6 23.4 %shard_map.186 = (bf16[3,800,128]{2,1,0:T(8,128)(2,1)S(1)}, bf16[3,800,128]{2,1,0:T(8,128)(2,1)S(1)}, bf16[3072,128]{1,0:T(8,128)(2,1)S(1)}, bf16[3072,128]{1,0:T(8,128)(2,1)S(1)}) custom-call(bf16[768,128]{1,0:T(8,128)(2,1)S(1)} %constant_dynamic-update-slice_fusion.refs_0_, bf16[768,128]{1,0:T(8,128)(2,1)S(1)} %collective-permute-done.4.refs_1_, ...), custom_call_target="tpu_custom_call" | custom-call | flops 7247757312 | bytes 4000000 | tf_op jit(solution)/shard_map/pallas_call | solution.py:34
  165.4 8.2 %shard_map.187 = (bf16[800,128]{1,0:T(8,128)(2,1)S(1)}, bf16[800,128]{1,0:T(8,128)(2,1)S(1)}) custom-call(bf16[768,128]{1,0:T(8,128)(2,1)S(1)} %constant_dynamic-update-slice_fusion.refs_0_, bf16[3072,128]{1,0:T(8,128)(2,1)S(1)} %get-tuple-element.26.refs_1_, bf16[3072,128]{1,0:T(8,128)(2,1)S(1)} %get-tuple-element.27.refs_2_), custom_call_target="tpu_custom_call" | custom-call | flops 2415919104 | bytes 4000000 | tf_op jit(solution)/shard_map/pallas_call | solution.py:34
  174.9 3.7 %collective-permute-start.16 = (bf16[800,128]{1,0:T(8,128)(2,1)S(1)}, bf16[800,128]{1,0:T(8,128)(2,1)S(1)}, u32[]{:S(2)}, u32[]{:S(2)}) collective-permute-start(bf16[800,128]{1,0:T(8,128)(2,1)S(1)} %get-tuple-element.32), channel_id=1, source_target_pairs={{0,24},{8,0},{16,8},{24,16},{1,25},{9,1},{17,9},{25,17},{2,26},{10... | collective-permute-start | bytes 614408 | tf_op jit(solution)/shard_map/ppermute | solution.py:27
  181.1 2.9 %shard_map.190.hidden = bf16[384,128]{1,0:T(8,128)(2,1)S(1)} custom-call(bf16[352,2048]{1,0:T(8,128)(2,1)} %constant_dynamic-update-slice_fusion.2.x0, bf16[352,2048]{1,0:T(8,128)(2,1)S(1)} %collective-permute-done.19.x1, bf16[352,2048]{1,0:T(8,128)(2,1)S(1)} %collective-permute-done.20.x2, bf16[352,2048]{1,0:T(8,128)(2,1)S(1)} %collective-permute-done.21.x3, ...), custom_call_target="tpu_custom_call" | custom-call | flops 402653184 | bytes 3000000 | tf_op jit(solution)/shard_map/pallas_call | solution.py:34
  184.0 3.5 %collective-permute-done.16.p1 = bf16[800,128]{1,0:T(8,128)(2,1)S(1)} collective-permute-done((bf16[800,128]{1,0:T(8,128)(2,1)S(1)}, bf16[800,128]{1,0:T(8,128)(2,1)S(1)}, u32[]{:S(2)}, u32[]{:S(2)}) %collective-permute-start.16) | collective-permute-done | bytes 204832 | tf_op jit(solution)/shard_map/ppermute | solution.py:27
  187.5 3.4 %collective-permute-done.17.p2 = bf16[800,128]{1,0:T(8,128)(2,1)S(1)} collective-permute-done((bf16[800,128]{1,0:T(8,128)(2,1)S(1)}, bf16[800,128]{1,0:T(8,128)(2,1)S(1)}, u32[]{:S(2)}, u32[]{:S(2)}) %collective-permute-start.17) | collective-permute-done | bytes 204832 | tf_op jit(solution)/shard_map/ppermute | solution.py:27
  194.3 3.3 %collective-permute-start.24 = (bf16[192,128]{1,0:T(8,128)(2,1)}, bf16[192,128]{1,0:T(8,128)(2,1)}, u32[]{:S(2)}, u32[]{:S(2)}) collective-permute-start(bf16[192,128]{1,0:T(8,128)(2,1)} %get-tuple-element.40), channel_id=1, source_target_pairs={{0,2},{1,3},{2,0},{3,1},{4,6},{5,7},{6,4},{7,5},{8,10},{9,11},{10,... | collective-permute-start | bytes 147464 | tf_op jit(solution)/shard_map/ppermute | solution.py:27
  199.0 2.6 %shard_map.193.routed = f32[96,2048]{1,0:T(8,128)S(1)} custom-call(bf16[384,16,128]{2,1,0:T(8,128)(2,1)} %bitcast.5.ret, s32[192]{0:T(256)S(1)} %copy-done.16, f32[192]{0:T(256)S(1)} %copy-done.14), custom_call_target="tpu_custom_call" | custom-call | flops 10000000 | bytes 3000000 | tf_op jit(solution)/shard_map/pallas_call | solution.py:34
  201.7 2.6 %shard_map.194 = (bf16[96,2048]{1,0:T(8,128)(2,1)}, bf16[96,2048]{1,0:T(8,128)(2,1)}) custom-call(bf16[192,128]{1,0:T(8,128)(2,1)S(1)} %get-tuple-element.37.a0, bf16[192,128]{1,0:T(8,128)(2,1)S(1)} %collective-permute-done.22.a1, bf16[192,128]{1,0:T(8,128)(2,1)S(1)} %collective-permute-done.23.a2, bf16[192,128]{1,0:T(8,128)(2,1)} %collective-permute-done.24.a3, ...), custom_call_target="tpu_custom_call" | custom-call | flops 402653184 | bytes 8000000 | tf_op jit(solution)/shard_map/pallas_call | solution.py:34
  (98 shorter events, 34.4 us)
Async XLA Ops:
  7.5 50.9 %all-to-all-start = ((bf16[64,96,128]{2,1,0:T(8,128)(2,1)}), bf16[64,96,128]{2,1,0:T(8,128)(2,1)}, u32[]{:S(2)}, u32[]{:S(2)}) async-start(bf16[64,96,128]{2,1,0:T(8,128)(2,1)} %bitcast.2), calls=%async_computation | async-start | bytes 3145728 | tf_op jit(solution)/shard_map/all_to_all | solution.py:428
  20.1 11.3 %collective-permute-start = (bf16[96,2048]{1,0:T(8,128)(2,1)}, bf16[96,2048]{1,0:T(8,128)(2,1)S(1)}, u32[]{:S(2)}, u32[]{:S(2)}) collective-permute-start(bf16[96,2048]{1,0:T(8,128)(2,1)} %fusion.2.r0), channel_id=1, source_target_pairs={{0,1},{1,2},{2,3},{3,0},{4,5},{5,6},{6,7},{7,4},{8,9},{9,10},{10,1... | collective-permute-start | bytes 1179656 | tf_op jit(solution)/shard_map/ppermute | solution.py:27
  21.6 51.5 %collective-permute-start.1 = (bf16[96,2048]{1,0:T(8,128)(2,1)}, bf16[96,2048]{1,0:T(8,128)(2,1)}, u32[]{:S(2)}, u32[]{:S(2)}) collective-permute-start(bf16[96,2048]{1,0:T(8,128)(2,1)} %fusion.2.r0), channel_id=1, source_target_pairs={{0,3},{1,0},{2,1},{3,2},{4,7},{5,4},{6,5},{7,6},{8,11},{9,8},{10,9... | collective-permute-start | bytes 1179656 | tf_op jit(solution)/shard_map/ppermute | solution.py:27
  34.0 93.9 %collective-permute-start.20 = (bf16[352,2048]{1,0:T(8,128)(2,1)}, bf16[352,2048]{1,0:T(8,128)(2,1)S(1)}, u32[]{:S(2)}, u32[]{:S(2)}) collective-permute-start(bf16[352,2048]{1,0:T(8,128)(2,1)} %constant_dynamic-update-slice_fusion.2.x0), channel_id=1, source_target_pairs={{0,3},{1,0},{2,1},{3,2},{4,7},{5,4},{6,5},{7,6},{8,11},{9,8},{10,9... | collective-permute-start | bytes 4325384 | tf_op jit(solution)/shard_map/ppermute | solution.py:27
  35.8 94.8 %collective-permute-start.19 = (bf16[352,2048]{1,0:T(8,128)(2,1)}, bf16[352,2048]{1,0:T(8,128)(2,1)S(1)}, u32[]{:S(2)}, u32[]{:S(2)}) collective-permute-start(bf16[352,2048]{1,0:T(8,128)(2,1)} %constant_dynamic-update-slice_fusion.2.x0), channel_id=1, source_target_pairs={{0,1},{1,2},{2,3},{3,0},{4,5},{5,6},{6,7},{7,4},{8,9},{9,10},{10,1... | collective-permute-start | bytes 4325384 | tf_op jit(solution)/shard_map/ppermute | solution.py:27
  66.9 130.7 %all-to-all-start.1 = ((bf16[64,96,128]{2,1,0:T(8,128)(2,1)}), bf16[64,96,128]{2,1,0:T(8,128)(2,1)}, u32[]{:S(2)}, u32[]{:S(2)}) async-start(bf16[64,96,128]{2,1,0:T(8,128)(2,1)} %bitcast.8), calls=%async_computation.1 | async-start | bytes 3145728 | tf_op jit(solution)/shard_map/all_to_all | solution.py:476
  74.8 8.1 %collective-permute-start.2 = (bf16[96,2048]{1,0:T(8,128)(2,1)}, bf16[96,2048]{1,0:T(8,128)(2,1)}, u32[]{:S(2)}, u32[]{:S(2)}) collective-permute-start(bf16[96,2048]{1,0:T(8,128)(2,1)} %broadcast_select_fusion.1), channel_id=1, source_target_pairs={{0,1},{1,2},{2,3},{3,0},{4,7},{5,4},{6,5},{7,6},{8,9},{9,10},{10,1... | collective-permute-start | bytes 1179656 | tf_op jit(solution)/shard_map/ppermute | solution.py:51
  89.7 30.0 %collective-permute-start.10 = (bf16[384,256]{1,0:T(8,128)(2,1)S(1)}, bf16[384,256]{1,0:T(8,128)(2,1)S(1)}, u32[]{:S(2)}, u32[]{:S(2)}) collective-permute-start(bf16[384,256]{1,0:T(8,128)(2,1)S(1)} %get-tuple-element.25.refs_4_), channel_id=1, source_target_pairs={{0,192},{32,224},{64,0},{96,32},{128,64},{160,96},{192,128},{224,1... | collective-permute-start | bytes 589832 | tf_op jit(solution)/shard_map/ppermute | solution.py:27
  90.3 30.0 %collective-permute-start.9 = (bf16[384,256]{1,0:T(8,128)(2,1)S(1)}, bf16[384,256]{1,0:T(8,128)(2,1)S(1)}, u32[]{:S(2)}, u32[]{:S(2)}) collective-permute-start(bf16[384,256]{1,0:T(8,128)(2,1)S(1)} %get-tuple-element.25.refs_4_), channel_id=1, source_target_pairs={{0,64},{32,96},{64,128},{96,160},{128,192},{160,224},{192,0},{224,... | collective-permute-start | bytes 589832 | tf_op jit(solution)/shard_map/ppermute | solution.py:27
  95.2 28.2 %collective-permute-start.8 = (bf16[384,256]{1,0:T(8,128)(2,1)S(1)}, bf16[384,256]{1,0:T(8,128)(2,1)S(1)}, u32[]{:S(2)}, u32[]{:S(2)}) collective-permute-start(bf16[384,256]{1,0:T(8,128)(2,1)S(1)} %get-tuple-element.25.refs_4_), channel_id=1, source_target_pairs={{0,224},{32,0},{64,32},{96,64},{128,96},{160,128},{192,160},{224,1... | collective-permute-start | bytes 589832 | tf_op jit(solution)/shard_map/ppermute | solution.py:27
  120.3 7.6 %collective-permute-start.6 = (bf16[768,128]{1,0:T(8,128)(2,1)S(1)}, bf16[768,128]{1,0:T(8,128)(2,1)S(1)}, u32[]{:S(2)}, u32[]{:S(2)}) collective-permute-start(bf16[768,128]{1,0:T(8,128)(2,1)S(1)} %constant_dynamic-update-slice_fusion.refs_0_), channel_id=1, source_target_pairs={{0,16},{8,24},{16,0},{24,8},{1,17},{9,25},{17,1},{25,9},{2,18},{10... | collective-permute-start | bytes 589832 | tf_op jit(solution)/shard_map/ppermute | solution.py:27
  123.4 8.4 %collective-permute-start.5 = (bf16[768,128]{1,0:T(8,128)(2,1)S(1)}, bf16[768,128]{1,0:T(8,128)(2,1)S(1)}, u32[]{:S(2)}, u32[]{:S(2)}) collective-permute-start(bf16[768,128]{1,0:T(8,128)(2,1)S(1)} %constant_dynamic-update-slice_fusion.refs_0_), channel_id=1, source_target_pairs={{0,24},{8,0},{16,8},{24,16},{1,25},{9,1},{17,9},{25,17},{2,26},{10... | collective-permute-start | bytes 589832 | tf_op jit(solution)/shard_map/ppermute | solution.py:27
  125.4 8.0 %collective-permute-start.4 = (bf16[768,128]{1,0:T(8,128)(2,1)S(1)}, bf16[768,128]{1,0:T(8,128)(2,1)S(1)}, u32[]{:S(2)}, u32[]{:S(2)}) collective-permute-start(bf16[768,128]{1,0:T(8,128)(2,1)S(1)} %constant_dynamic-update-slice_fusion.refs_0_), channel_id=1, source_target_pairs={{0,8},{8,16},{16,24},{24,0},{1,9},{9,17},{17,25},{25,1},{2,10},{10... | collective-permute-start | bytes 589832 | tf_op jit(solution)/shard_map/ppermute | solution.py:27
  127.9 12.8 %collective-permute-start.13 = (bf16[384,256]{1,0:T(8,128)(2,1)S(1)}, bf16[384,256]{1,0:T(8,128)(2,1)S(1)}, u32[]{:S(2)}, u32[]{:S(2)}) collective-permute-start(bf16[384,256]{1,0:T(8,128)(2,1)S(1)} %collective-permute-done.10.refs_8_), channel_id=1, source_target_pairs={{0,192},{32,224},{64,0},{96,32},{128,64},{160,96},{192,128},{224,1... | collective-permute-start | bytes 589832 | tf_op jit(solution)/shard_map/ppermute | solution.py:27
  128.0 13.7 %collective-permute-start.12 = (bf16[384,256]{1,0:T(8,128)(2,1)S(1)}, bf16[384,256]{1,0:T(8,128)(2,1)S(1)}, u32[]{:S(2)}, u32[]{:S(2)}) collective-permute-start(bf16[384,256]{1,0:T(8,128)(2,1)S(1)} %collective-permute-done.10.refs_8_), channel_id=1, source_target_pairs={{0,224},{32,0},{64,32},{96,64},{128,96},{160,128},{192,160},{224,1... | collective-permute-start | bytes 589832 | tf_op jit(solution)/shard_map/ppermute | solution.py:27
  130.6 11.0 %collective-permute-start.11 = (bf16[384,256]{1,0:T(8,128)(2,1)S(1)}, bf16[384,256]{1,0:T(8,128)(2,1)S(1)}, u32[]{:S(2)}, u32[]{:S(2)}) collective-permute-start(bf16[384,256]{1,0:T(8,128)(2,1)S(1)} %collective-permute-done.9.refs_7_), channel_id=1, source_target_pairs={{0,32},{32,64},{64,96},{96,128},{128,160},{160,192},{192,224},{224... | collective-permute-start | bytes 589832 | tf_op jit(solution)/shard_map/ppermute | solution.py:27
  131.8 49.2 %collective-permute-start.21 = (bf16[352,2048]{1,0:T(8,128)(2,1)S(1)}, bf16[352,2048]{1,0:T(8,128)(2,1)S(1)}, u32[]{:S(2)}, u32[]{:S(2)}) collective-permute-start(bf16[352,2048]{1,0:T(8,128)(2,1)S(1)} %broadcast_select_fusion), channel_id=1, source_target_pairs={{0,1},{1,2},{2,3},{3,0},{4,7},{5,4},{6,5},{7,6},{8,9},{9,10},{10,1... | collective-permute-start | bytes 4325384 | tf_op jit(solution)/shard_map/ppermute | solution.py:51
  165.0 9.1 %collective-permute-start.15 = (bf16[3,800,128]{2,1,0:T(8,128)(2,1)S(1)}, bf16[3,800,128]{2,1,0:T(8,128)(2,1)S(1)}, u32[]{:S(2)}, u32[]{:S(2)}) collective-permute-start(bf16[3,800,128]{2,1,0:T(8,128)(2,1)S(1)} %get-tuple-element.31), channel_id=1, source_target_pairs={{0,4},{4,0},{1,5},{5,1},{2,6},{6,2},{3,7},{7,3},{8,12},{12,8},{9,1... | collective-permute-start | bytes 1843208 | tf_op jit(solution)/shard_map/ppermute | solution.py:27
  173.6 10.4 %collective-permute-start.14 = (bf16[800,128]{1,0:T(8,128)(2,1)S(1)}, bf16[800,128]{1,0:T(8,128)(2,1)S(1)}, u32[]{:S(2)}, u32[]{:S(2)}) collective-permute-start(bf16[800,128]{1,0:T(8,128)(2,1)S(1)} %get-tuple-element.29), channel_id=1, source_target_pairs={{0,4},{4,0},{1,5},{5,1},{2,6},{6,2},{3,7},{7,3},{8,12},{12,8},{9,1... | collective-permute-start | bytes 614408 | tf_op jit(solution)/shard_map/ppermute | solution.py:27
  174.9 12.6 %collective-permute-start.16 = (bf16[800,128]{1,0:T(8,128)(2,1)S(1)}, bf16[800,128]{1,0:T(8,128)(2,1)S(1)}, u32[]{:S(2)}, u32[]{:S(2)}) collective-permute-start(bf16[800,128]{1,0:T(8,128)(2,1)S(1)} %get-tuple-element.32), channel_id=1, source_target_pairs={{0,24},{8,0},{16,8},{24,16},{1,25},{9,1},{17,9},{25,17},{2,26},{10... | collective-permute-start | bytes 614408 | tf_op jit(solution)/shard_map/ppermute | solution.py:27
  178.6 12.3 %collective-permute-start.17 = (bf16[800,128]{1,0:T(8,128)(2,1)S(1)}, bf16[800,128]{1,0:T(8,128)(2,1)S(1)}, u32[]{:S(2)}, u32[]{:S(2)}) collective-permute-start(bf16[800,128]{1,0:T(8,128)(2,1)S(1)} %get-tuple-element.33), channel_id=1, source_target_pairs={{0,8},{8,16},{16,24},{24,0},{1,9},{9,17},{17,25},{25,1},{2,10},{10... | collective-permute-start | bytes 614408 | tf_op jit(solution)/shard_map/ppermute | solution.py:27
  178.6 12.3 %collective-permute-start.18 = (bf16[800,128]{1,0:T(8,128)(2,1)S(1)}, bf16[800,128]{1,0:T(8,128)(2,1)S(1)}, u32[]{:S(2)}, u32[]{:S(2)}) collective-permute-start(bf16[800,128]{1,0:T(8,128)(2,1)S(1)} %get-tuple-element.34), channel_id=1, source_target_pairs={{0,16},{8,24},{16,0},{24,8},{1,17},{9,25},{17,1},{25,9},{2,18},{10... | collective-permute-start | bytes 614408 | tf_op jit(solution)/shard_map/ppermute | solution.py:27
  192.2 9.4 %collective-permute-start.22 = (bf16[192,128]{1,0:T(8,128)(2,1)}, bf16[192,128]{1,0:T(8,128)(2,1)S(1)}, u32[]{:S(2)}, u32[]{:S(2)}) collective-permute-start(bf16[192,128]{1,0:T(8,128)(2,1)} %get-tuple-element.38), channel_id=1, source_target_pairs={{0,3},{1,0},{2,1},{3,2},{4,7},{5,4},{6,5},{7,6},{8,11},{9,8},{10,9... | collective-permute-start | bytes 147464 | tf_op jit(solution)/shard_map/ppermute | solution.py:27
  192.8 8.9 %collective-permute-start.23 = (bf16[192,128]{1,0:T(8,128)(2,1)}, bf16[192,128]{1,0:T(8,128)(2,1)S(1)}, u32[]{:S(2)}, u32[]{:S(2)}) collective-permute-start(bf16[192,128]{1,0:T(8,128)(2,1)} %get-tuple-element.39), channel_id=1, source_target_pairs={{0,1},{1,2},{2,3},{3,0},{4,5},{5,6},{6,7},{7,4},{8,9},{9,10},{10,1... | collective-permute-start | bytes 147464 | tf_op jit(solution)/shard_map/ppermute | solution.py:27
  (24 other events, 121.3 us)

commit v2 on v1

--- a/solution.py
+++ b/solution.py
@@ -331,7 +331,7 @@
         row = xf[t]
         for k in range(top_count):
             i = t * top_count + k
-            e = routes[i]
+            e = routes[k, t]
             c = count[e]
             count[e] = c + 1
             s = e * capacity + c
@@ -339,7 +339,7 @@
             out[s] = row
         return carry
 
-    lax.fori_loop(0, x_ref.shape[0], step, 0)
+    lax.fori_loop(0, x_ref.shape[0], step, 0, unroll=4)
 
 
 def combine_kernel(top_count, ret, slots, shares, out, tiles):
@@ -349,12 +349,12 @@
         acc = None
         for k in range(top_count):
             i = t * top_count + k
-            v = ret[slots[i]].astype(F32) * shares[i]
+            v = ret[slots[i]].astype(F32) * shares[k, t]
             acc = v if acc is None else acc + v
         tiles[pl.ds(pl.multiple_of(t * subs, subs), subs), :] = acc
         return carry
 
-    lax.fori_loop(0, out.shape[0], step, 0)
+    lax.fori_loop(0, out.shape[0], step, 0, unroll=4)
     from_tiles(tiles, out)
 
 
@@ -402,13 +402,12 @@
         vmem=12,
     )
 
-    flat_routes = routes.reshape(-1)
     outgoing, normed_expert, slot_index = call(
         functools.partial(dispatch_kernel, capacity, top_count),
         [
             (expert_in, VMEM),
             (expert_gain.reshape(1, width), VMEM),
-            (flat_routes, SMEM),
+            (routes.T, SMEM),
         ],
         [
             S((slots_all, subs, lanes), BF),
@@ -430,7 +429,7 @@
     )
 
     shares = ROUTED_SCALE * route_weights / jnp.sum(route_weights, axis=1, keepdims=True)
-    queries, shares = lax.optimization_barrier((queries, shares.reshape(-1)))
+    queries, shares = lax.optimization_barrier((queries, shares.T))
 
     near = [shift(kv, "ep_0", k) for k in (1, -1, 2, -2)]
     far = [shift(near[2], "ep_0", 1), shift(near[3], "ep_0", -1)]

time: 205 us -> 204 us (level)
  the two profiles are of different devices: /device:TPU:66 before, /device:TPU:22 now
where the time goes in v2:
time: 204 us; the launch traced here: 200 us
  waiting for transfers between devices  80.5 us (39%)
  Pallas kernels  55.7 us (27%)
  starting transfers between devices  47.9 us (23%)
  local copies, waits for them, and re-layouts  11 us (5%)
  other arithmetic  3.61 us (2%)
    pallas_call x10, Pallas kernels, call(): pl.pallas_call(kernel, out_shape=outs[0] if single else outs, in_specs=[s...  55.7 us
    ppermute x23, waiting for transfers between devices, shift(): return lax.ppermute(x, axis, [(i, (i + k) % n) for i in range(n)])  51.8 us
    ppermute x23, starting transfers between devices, shift(): return lax.ppermute(x, axis, [(i, (i + k) % n) for i in range(n)])  29.1 us
    all_to_all x1, waiting for transfers between devices, on_device(): lax.all_to_all(outgoing.reshape(experts, capacity * subs, lanes), EP, 0,...  21.7 us
    all_to_all x1, starting transfers between devices, on_device(): lax.all_to_all(outgoing.reshape(experts, capacity * subs, lanes), EP, 0,...  12.2 us
    unnamed x47, local copies, waits for them, and re-layouts  10.2 us
    ppermute x2, waiting for transfers between devices, forward_by_core(): lax.ppermute(picked, ('ep_2', axis) if last else (axis, 'ep_2'), pairs)  7.05 us
    all_to_all x1, starting transfers between devices, on_device(): lax.all_to_all(result.reshape(experts, capacity * subs, lanes), EP, 0, 0,...  5.59 us
  transfers between devices with their start and end apart: 27, of which 12 were waited for; matrix products, arithmetic and copies ran while one was open for 3% of the time, Pallas kernels for 25%

profile of v2, /device:TPU:22, one launch (start us, length us, event | category | flops | bytes accessed | tf_op | source)
XLA Modules:
  0.0 200.3 jit_solution(12129634714671976283)
XLA Ops:
  3.0 3.3 %shard_map.189 = (bf16[384,16,128]{2,1,0:T(8,128)(2,1)}, bf16[96,2048]{1,0:T(8,128)(2,1)S(1)}, s32[192]{0:T(256)S(1)}) custom-call(bf16[96,2048]{1,0:T(8,128)(2,1)S(1)} %copy-done.12, f32[1,2048]{1,0:T(1,128)S(1)} %bitcast.9, s32[2,96]{1,0:T(2,128)S(1)} %bitcast.10), custom_call_target="tpu_custom_call" | custom-call | flops 10000000 | bytes 2000000 | tf_op jit(solution)/shard_map/pallas_call | solution.py:34
  6.8 12.2 %all-to-all-start = ((bf16[64,96,128]{2,1,0:T(8,128)(2,1)}), bf16[64,96,128]{2,1,0:T(8,128)(2,1)}, u32[]{:S(2)}, u32[]{:S(2)}) async-start(bf16[64,96,128]{2,1,0:T(8,128)(2,1)} %bitcast.4), calls=%async_computation | async-start | bytes 3145728 | tf_op jit(solution)/shard_map/all_to_all | solution.py:427
  22.1 9.3 %collective-permute-done.r1 = bf16[96,2048]{1,0:T(8,128)(2,1)S(1)} collective-permute-done((bf16[96,2048]{1,0:T(8,128)(2,1)}, bf16[96,2048]{1,0:T(8,128)(2,1)S(1)}, u32[]{:S(2)}, u32[]{:S(2)}) %collective-permute-start) | collective-permute-done | bytes 393248 | tf_op jit(solution)/shard_map/ppermute | solution.py:27
  34.8 2.4 %collective-permute-start.19 = (bf16[352,2048]{1,0:T(8,128)(2,1)}, bf16[352,2048]{1,0:T(8,128)(2,1)S(1)}, u32[]{:S(2)}, u32[]{:S(2)}) collective-permute-start(bf16[352,2048]{1,0:T(8,128)(2,1)} %constant_dynamic-update-slice_fusion.2.x0), channel_id=1, source_target_pairs={{0,1},{1,2},{2,3},{3,0},{4,5},{5,6},{6,7},{7,4},{8,9},{9,10},{10,1... | collective-permute-start | bytes 4325384 | tf_op jit(solution)/shard_map/ppermute | solution.py:27
  37.3 21.7 %all-to-all-done = bf16[64,96,128]{2,1,0:T(8,128)(2,1)} async-done(((bf16[64,96,128]{2,1,0:T(8,128)(2,1)}), bf16[64,96,128]{2,1,0:T(8,128)(2,1)}, u32[]{:S(2)}, u32[]{:S(2)}) %all-to-all-start) | async-done | bytes 1572896 | tf_op jit(solution)/shard_map/all_to_all | solution.py:427
  58.9 8.5 %shard_map.192 = bf16[384,16,128]{2,1,0:T(8,128)(2,1)} custom-call(bf16[384,16,128]{2,1,0:T(8,128)(2,1)} %bitcast.5.x_ref, bf16[1,2048,512]{2,1,0:T(8,128)(2,1)} %refs_0_.1, bf16[1,2048,512]{2,1,0:T(8,128)(2,1)} %refs_1_.1, bf16[1,512,2048]{2,1,0:T(8,128)(2,1)} %refs_2_.1), custom_call_target="tpu_custom_call" | custom-call | flops 2415919104 | bytes 10000000 | tf_op jit(solution)/shard_map/pallas_call | solution.py:34
  67.4 5.6 %all-to-all-start.1 = ((bf16[64,96,128]{2,1,0:T(8,128)(2,1)}), bf16[64,96,128]{2,1,0:T(8,128)(2,1)}, u32[]{:S(2)}, u32[]{:S(2)}) async-start(bf16[64,96,128]{2,1,0:T(8,128)(2,1)} %bitcast.12), calls=%async_computation.1 | async-start | bytes 3145728 | tf_op jit(solution)/shard_map/all_to_all | solution.py:475
  75.9 7.0 %collective-permute-done.2.r3 = bf16[96,2048]{1,0:T(8,128)(2,1)} collective-permute-done((bf16[96,2048]{1,0:T(8,128)(2,1)}, bf16[96,2048]{1,0:T(8,128)(2,1)}, u32[]{:S(2)}, u32[]{:S(2)}) %collective-permute-start.2) | collective-permute-done | bytes 393248 | tf_op jit(solution)/shard_map/ppermute | solution.py:51
  87.1 2.6 %shard_map.185 = (bf16[384,128]{1,0:T(8,128)(2,1)S(1)}, bf16[384,256]{1,0:T(8,128)(2,1)S(1)}) custom-call(bf16[96,2048]{1,0:T(8,128)(2,1)} %fusion.2.r0, bf16[96,2048]{1,0:T(8,128)(2,1)S(1)} %copy-done.6, bf16[96,2048]{1,0:T(8,128)(2,1)} %collective-permute-done.1.r2, bf16[96,2048]{1,0:T(8,128)(2,1)} %collective-permute-done.2.r3, ...), custom_call_target="tpu_custom_call" | custom-call | flops 603979776 | bytes 4000000 | tf_op jit(solution)/shard_map/pallas_call | solution.py:34
  89.7 3.9 %collective-permute-start.10 = (bf16[384,256]{1,0:T(8,128)(2,1)S(1)}, bf16[384,256]{1,0:T(8,128)(2,1)S(1)}, u32[]{:S(2)}, u32[]{:S(2)}) collective-permute-start(bf16[384,256]{1,0:T(8,128)(2,1)S(1)} %get-tuple-element.25.refs_4_), channel_id=1, source_target_pairs={{0,192},{32,224},{64,0},{96,32},{128,64},{160,96},{192,128},{224,1... | collective-permute-start | bytes 589832 | tf_op jit(solution)/shard_map/ppermute | solution.py:27
  94.9 3.3 %collective-permute-start.8 = (bf16[384,256]{1,0:T(8,128)(2,1)S(1)}, bf16[384,256]{1,0:T(8,128)(2,1)S(1)}, u32[]{:S(2)}, u32[]{:S(2)}) collective-permute-start(bf16[384,256]{1,0:T(8,128)(2,1)S(1)} %get-tuple-element.25.refs_4_), channel_id=1, source_target_pairs={{0,224},{32,0},{64,32},{96,64},{128,96},{160,128},{192,160},{224,1... | collective-permute-start | bytes 589832 | tf_op jit(solution)/shard_map/ppermute | solution.py:27
  98.2 20.6 %collective-permute-done.10.refs_8_ = bf16[384,256]{1,0:T(8,128)(2,1)S(1)} collective-permute-done((bf16[384,256]{1,0:T(8,128)(2,1)S(1)}, bf16[384,256]{1,0:T(8,128)(2,1)S(1)}, u32[]{:S(2)}, u32[]{:S(2)}) %collective-permute-start.10) | collective-permute-done | bytes 196640 | tf_op jit(solution)/shard_map/ppermute | solution.py:27
  122.1 3.6 %collective-permute-done.7.refs_5_ = bf16[384,256]{1,0:T(8,128)(2,1)S(1)} collective-permute-done((bf16[384,256]{1,0:T(8,128)(2,1)S(1)}, bf16[384,256]{1,0:T(8,128)(2,1)S(1)}, u32[]{:S(2)}, u32[]{:S(2)}) %collective-permute-start.7) | collective-permute-done | bytes 196640 | tf_op jit(solution)/shard_map/ppermute | solution.py:27
  126.8 3.5 %collective-permute-start.13 = (bf16[384,256]{1,0:T(8,128)(2,1)S(1)}, bf16[384,256]{1,0:T(8,128)(2,1)S(1)}, u32[]{:S(2)}, u32[]{:S(2)}) collective-permute-start(bf16[384,256]{1,0:T(8,128)(2,1)S(1)} %collective-permute-done.10.refs_8_), channel_id=1, source_target_pairs={{0,192},{32,224},{64,0},{96,32},{128,64},{160,96},{192,128},{224,1... | collective-permute-start | bytes 589832 | tf_op jit(solution)/shard_map/ppermute | solution.py:27
  133.3 4.4 %collective-permute-done.13.refs_11_ = bf16[384,256]{1,0:T(8,128)(2,1)S(1)} collective-permute-done((bf16[384,256]{1,0:T(8,128)(2,1)S(1)}, bf16[384,256]{1,0:T(8,128)(2,1)S(1)}, u32[]{:S(2)}, u32[]{:S(2)}) %collective-permute-start.13) | collective-permute-done | bytes 196640 | tf_op jit(solution)/shard_map/ppermute | solution.py:27
  137.7 3.9 %collective-permute-done.12.refs_10_ = bf16[384,256]{1,0:T(8,128)(2,1)S(1)} collective-permute-done((bf16[384,256]{1,0:T(8,128)(2,1)S(1)}, bf16[384,256]{1,0:T(8,128)(2,1)S(1)}, u32[]{:S(2)}, u32[]{:S(2)}) %collective-permute-start.12) | collective-permute-done | bytes 196640 | tf_op jit(solution)/shard_map/ppermute | solution.py:27
  141.6 23.4 %shard_map.186 = (bf16[3,800,128]{2,1,0:T(8,128)(2,1)S(1)}, bf16[3,800,128]{2,1,0:T(8,128)(2,1)S(1)}, bf16[3072,128]{1,0:T(8,128)(2,1)S(1)}, bf16[3072,128]{1,0:T(8,128)(2,1)S(1)}) custom-call(bf16[768,128]{1,0:T(8,128)(2,1)S(1)} %constant_dynamic-update-slice_fusion.refs_0_, bf16[768,128]{1,0:T(8,128)(2,1)S(1)} %collective-permute-done.4.refs_1_, ...), custom_call_target="tpu_custom_call" | custom-call | flops 7247757312 | bytes 4000000 | tf_op jit(solution)/shard_map/pallas_call | solution.py:34
  165.4 8.2 %shard_map.187 = (bf16[800,128]{1,0:T(8,128)(2,1)S(1)}, bf16[800,128]{1,0:T(8,128)(2,1)S(1)}) custom-call(bf16[768,128]{1,0:T(8,128)(2,1)S(1)} %constant_dynamic-update-slice_fusion.refs_0_, bf16[3072,128]{1,0:T(8,128)(2,1)S(1)} %get-tuple-element.26.refs_1_, bf16[3072,128]{1,0:T(8,128)(2,1)S(1)} %get-tuple-element.27.refs_2_), custom_call_target="tpu_custom_call" | custom-call | flops 2415919104 | bytes 4000000 | tf_op jit(solution)/shard_map/pallas_call | solution.py:34
  178.6 2.9 %shard_map.190.hidden = bf16[384,128]{1,0:T(8,128)(2,1)S(1)} custom-call(bf16[352,2048]{1,0:T(8,128)(2,1)} %constant_dynamic-update-slice_fusion.2.x0, bf16[352,2048]{1,0:T(8,128)(2,1)S(1)} %collective-permute-done.19.x1, bf16[352,2048]{1,0:T(8,128)(2,1)S(1)} %collective-permute-done.20.x2, bf16[352,2048]{1,0:T(8,128)(2,1)S(1)} %collective-permute-done.21.x3, ...), custom_call_target="tpu_custom_call" | custom-call | flops 402653184 | bytes 3000000 | tf_op jit(solution)/shard_map/pallas_call | solution.py:34
  182.9 4.3 %collective-permute-done.18.p3 = bf16[800,128]{1,0:T(8,128)(2,1)S(1)} collective-permute-done((bf16[800,128]{1,0:T(8,128)(2,1)S(1)}, bf16[800,128]{1,0:T(8,128)(2,1)S(1)}, u32[]{:S(2)}, u32[]{:S(2)}) %collective-permute-start.18) | collective-permute-done | bytes 204832 | tf_op jit(solution)/shard_map/ppermute | solution.py:27
  189.4 2.4 %collective-permute-start.23 = (bf16[192,128]{1,0:T(8,128)(2,1)}, bf16[192,128]{1,0:T(8,128)(2,1)S(1)}, u32[]{:S(2)}, u32[]{:S(2)}) collective-permute-start(bf16[192,128]{1,0:T(8,128)(2,1)} %get-tuple-element.39), channel_id=1, source_target_pairs={{0,1},{1,2},{2,3},{3,0},{4,5},{5,6},{6,7},{7,4},{8,9},{9,10},{10,1... | collective-permute-start | bytes 147464 | tf_op jit(solution)/shard_map/ppermute | solution.py:27
  193.4 2.2 %shard_map.193.routed = f32[96,2048]{1,0:T(8,128)S(1)} custom-call(bf16[384,16,128]{2,1,0:T(8,128)(2,1)} %bitcast.7.ret, s32[192]{0:T(256)S(1)} %copy-done.17, f32[2,96]{1,0:T(2,128)S(1)} %copy-done.14), custom_call_target="tpu_custom_call" | custom-call | flops 10000000 | bytes 3000000 | tf_op jit(solution)/shard_map/pallas_call | solution.py:34
  195.6 2.1 %collective-permute-done.24.a3 = bf16[192,128]{1,0:T(8,128)(2,1)} collective-permute-done((bf16[192,128]{1,0:T(8,128)(2,1)}, bf16[192,128]{1,0:T(8,128)(2,1)}, u32[]{:S(2)}, u32[]{:S(2)}) %collective-permute-start.24) | collective-permute-done | bytes 49184 | tf_op jit(solution)/shard_map/ppermute | solution.py:27
  197.7 2.6 %shard_map.194 = (bf16[96,2048]{1,0:T(8,128)(2,1)}, bf16[96,2048]{1,0:T(8,128)(2,1)}) custom-call(bf16[192,128]{1,0:T(8,128)(2,1)S(1)} %get-tuple-element.37.a0, bf16[192,128]{1,0:T(8,128)(2,1)S(1)} %collective-permute-done.22.a1, bf16[192,128]{1,0:T(8,128)(2,1)S(1)} %collective-permute-done.23.a2, bf16[192,128]{1,0:T(8,128)(2,1)} %collective-permute-done.24.a3, ...), custom_call_target="tpu_custom_call" | custom-call | flops 402653184 | bytes 8000000 | tf_op jit(solution)/shard_map/pallas_call | solution.py:34
  (96 shorter events, 34.9 us)
Async XLA Ops:
  6.8 52.1 %all-to-all-start = ((bf16[64,96,128]{2,1,0:T(8,128)(2,1)}), bf16[64,96,128]{2,1,0:T(8,128)(2,1)}, u32[]{:S(2)}, u32[]{:S(2)}) async-start(bf16[64,96,128]{2,1,0:T(8,128)(2,1)} %bitcast.4), calls=%async_computation | async-start | bytes 3145728 | tf_op jit(solution)/shard_map/all_to_all | solution.py:427
  20.1 11.3 %collective-permute-start = (bf16[96,2048]{1,0:T(8,128)(2,1)}, bf16[96,2048]{1,0:T(8,128)(2,1)S(1)}, u32[]{:S(2)}, u32[]{:S(2)}) collective-permute-start(bf16[96,2048]{1,0:T(8,128)(2,1)} %fusion.2.r0), channel_id=1, source_target_pairs={{0,1},{1,2},{2,3},{3,0},{4,5},{5,6},{6,7},{7,4},{8,9},{9,10},{10,1... | collective-permute-start | bytes 1179656 | tf_op jit(solution)/shard_map/ppermute | solution.py:27
  20.6 52.5 %collective-permute-start.1 = (bf16[96,2048]{1,0:T(8,128)(2,1)}, bf16[96,2048]{1,0:T(8,128)(2,1)}, u32[]{:S(2)}, u32[]{:S(2)}) collective-permute-start(bf16[96,2048]{1,0:T(8,128)(2,1)} %fusion.2.r0), channel_id=1, source_target_pairs={{0,3},{1,0},{2,1},{3,2},{4,7},{5,4},{6,5},{7,6},{8,11},{9,8},{10,9... | collective-permute-start | bytes 1179656 | tf_op jit(solution)/shard_map/ppermute | solution.py:27
  34.0 96.3 %collective-permute-start.20 = (bf16[352,2048]{1,0:T(8,128)(2,1)}, bf16[352,2048]{1,0:T(8,128)(2,1)S(1)}, u32[]{:S(2)}, u32[]{:S(2)}) collective-permute-start(bf16[352,2048]{1,0:T(8,128)(2,1)} %constant_dynamic-update-slice_fusion.2.x0), channel_id=1, source_target_pairs={{0,3},{1,0},{2,1},{3,2},{4,7},{5,4},{6,5},{7,6},{8,11},{9,8},{10,9... | collective-permute-start | bytes 4325384 | tf_op jit(solution)/shard_map/ppermute | solution.py:27
  34.8 96.4 %collective-permute-start.19 = (bf16[352,2048]{1,0:T(8,128)(2,1)}, bf16[352,2048]{1,0:T(8,128)(2,1)S(1)}, u32[]{:S(2)}, u32[]{:S(2)}) collective-permute-start(bf16[352,2048]{1,0:T(8,128)(2,1)} %constant_dynamic-update-slice_fusion.2.x0), channel_id=1, source_target_pairs={{0,1},{1,2},{2,3},{3,0},{4,5},{5,6},{6,7},{7,4},{8,9},{9,10},{10,1... | collective-permute-start | bytes 4325384 | tf_op jit(solution)/shard_map/ppermute | solution.py:27
  67.4 124.6 %all-to-all-start.1 = ((bf16[64,96,128]{2,1,0:T(8,128)(2,1)}), bf16[64,96,128]{2,1,0:T(8,128)(2,1)}, u32[]{:S(2)}, u32[]{:S(2)}) async-start(bf16[64,96,128]{2,1,0:T(8,128)(2,1)} %bitcast.12), calls=%async_computation.1 | async-start | bytes 3145728 | tf_op jit(solution)/shard_map/all_to_all | solution.py:475
  74.9 8.1 %collective-permute-start.2 = (bf16[96,2048]{1,0:T(8,128)(2,1)}, bf16[96,2048]{1,0:T(8,128)(2,1)}, u32[]{:S(2)}, u32[]{:S(2)}) collective-permute-start(bf16[96,2048]{1,0:T(8,128)(2,1)} %broadcast_select_fusion.1), channel_id=1, source_target_pairs={{0,1},{1,2},{2,3},{3,0},{4,7},{5,4},{6,5},{7,6},{8,9},{9,10},{10,1... | collective-permute-start | bytes 1179656 | tf_op jit(solution)/shard_map/ppermute | solution.py:51
  89.7 29.1 %collective-permute-start.10 = (bf16[384,256]{1,0:T(8,128)(2,1)S(1)}, bf16[384,256]{1,0:T(8,128)(2,1)S(1)}, u32[]{:S(2)}, u32[]{:S(2)}) collective-permute-start(bf16[384,256]{1,0:T(8,128)(2,1)S(1)} %get-tuple-element.25.refs_4_), channel_id=1, source_target_pairs={{0,192},{32,224},{64,0},{96,32},{128,64},{160,96},{192,128},{224,1... | collective-permute-start | bytes 589832 | tf_op jit(solution)/shard_map/ppermute | solution.py:27
  93.6 25.2 %collective-permute-start.9 = (bf16[384,256]{1,0:T(8,128)(2,1)S(1)}, bf16[384,256]{1,0:T(8,128)(2,1)S(1)}, u32[]{:S(2)}, u32[]{:S(2)}) collective-permute-start(bf16[384,256]{1,0:T(8,128)(2,1)S(1)} %get-tuple-element.25.refs_4_), channel_id=1, source_target_pairs={{0,64},{32,96},{64,128},{96,160},{128,192},{160,224},{192,0},{224,... | collective-permute-start | bytes 589832 | tf_op jit(solution)/shard_map/ppermute | solution.py:27
  94.9 26.6 %collective-permute-start.8 = (bf16[384,256]{1,0:T(8,128)(2,1)S(1)}, bf16[384,256]{1,0:T(8,128)(2,1)S(1)}, u32[]{:S(2)}, u32[]{:S(2)}) collective-permute-start(bf16[384,256]{1,0:T(8,128)(2,1)S(1)} %get-tuple-element.25.refs_4_), channel_id=1, source_target_pairs={{0,224},{32,0},{64,32},{96,64},{128,96},{160,128},{192,160},{224,1... | collective-permute-start | bytes 589832 | tf_op jit(solution)/shard_map/ppermute | solution.py:27
  118.8 6.9 %collective-permute-start.7 = (bf16[384,256]{1,0:T(8,128)(2,1)S(1)}, bf16[384,256]{1,0:T(8,128)(2,1)S(1)}, u32[]{:S(2)}, u32[]{:S(2)}) collective-permute-start(bf16[384,256]{1,0:T(8,128)(2,1)S(1)} %get-tuple-element.25.refs_4_), channel_id=1, source_target_pairs={{0,32},{32,64},{64,96},{96,128},{128,160},{160,192},{192,224},{224... | collective-permute-start | bytes 589832 | tf_op jit(solution)/shard_map/ppermute | solution.py:27
  118.8 8.1 %collective-permute-start.6 = (bf16[768,128]{1,0:T(8,128)(2,1)S(1)}, bf16[768,128]{1,0:T(8,128)(2,1)S(1)}, u32[]{:S(2)}, u32[]{:S(2)}) collective-permute-start(bf16[768,128]{1,0:T(8,128)(2,1)S(1)} %constant_dynamic-update-slice_fusion.refs_0_), channel_id=1, source_target_pairs={{0,16},{8,24},{16,0},{24,8},{1,17},{9,25},{17,1},{25,9},{2,18},{10... | collective-permute-start | bytes 589832 | tf_op jit(solution)/shard_map/ppermute | solution.py:27
  121.5 11.3 %collective-permute-start.5 = (bf16[768,128]{1,0:T(8,128)(2,1)S(1)}, bf16[768,128]{1,0:T(8,128)(2,1)S(1)}, u32[]{:S(2)}, u32[]{:S(2)}) collective-permute-start(bf16[768,128]{1,0:T(8,128)(2,1)S(1)} %constant_dynamic-update-slice_fusion.refs_0_), channel_id=1, source_target_pairs={{0,24},{8,0},{16,8},{24,16},{1,25},{9,1},{17,9},{25,17},{2,26},{10... | collective-permute-start | bytes 589832 | tf_op jit(solution)/shard_map/ppermute | solution.py:27
  125.7 7.6 %collective-permute-start.4 = (bf16[768,128]{1,0:T(8,128)(2,1)S(1)}, bf16[768,128]{1,0:T(8,128)(2,1)S(1)}, u32[]{:S(2)}, u32[]{:S(2)}) collective-permute-start(bf16[768,128]{1,0:T(8,128)(2,1)S(1)} %constant_dynamic-update-slice_fusion.refs_0_), channel_id=1, source_target_pairs={{0,8},{8,16},{16,24},{24,0},{1,9},{9,17},{17,25},{25,1},{2,10},{10... | collective-permute-start | bytes 589832 | tf_op jit(solution)/shard_map/ppermute | solution.py:27
  126.8 10.9 %collective-permute-start.13 = (bf16[384,256]{1,0:T(8,128)(2,1)S(1)}, bf16[384,256]{1,0:T(8,128)(2,1)S(1)}, u32[]{:S(2)}, u32[]{:S(2)}) collective-permute-start(bf16[384,256]{1,0:T(8,128)(2,1)S(1)} %collective-permute-done.10.refs_8_), channel_id=1, source_target_pairs={{0,192},{32,224},{64,0},{96,32},{128,64},{160,96},{192,128},{224,1... | collective-permute-start | bytes 589832 | tf_op jit(solution)/shard_map/ppermute | solution.py:27
  130.3 11.3 %collective-permute-start.12 = (bf16[384,256]{1,0:T(8,128)(2,1)S(1)}, bf16[384,256]{1,0:T(8,128)(2,1)S(1)}, u32[]{:S(2)}, u32[]{:S(2)}) collective-permute-start(bf16[384,256]{1,0:T(8,128)(2,1)S(1)} %collective-permute-done.10.refs_8_), channel_id=1, source_target_pairs={{0,224},{32,0},{64,32},{96,64},{128,96},{160,128},{192,160},{224,1... | collective-permute-start | bytes 589832 | tf_op jit(solution)/shard_map/ppermute | solution.py:27
  131.3 10.4 %collective-permute-start.11 = (bf16[384,256]{1,0:T(8,128)(2,1)S(1)}, bf16[384,256]{1,0:T(8,128)(2,1)S(1)}, u32[]{:S(2)}, u32[]{:S(2)}) collective-permute-start(bf16[384,256]{1,0:T(8,128)(2,1)S(1)} %collective-permute-done.9.refs_7_), channel_id=1, source_target_pairs={{0,32},{32,64},{64,96},{96,128},{128,160},{160,192},{192,224},{224... | collective-permute-start | bytes 589832 | tf_op jit(solution)/shard_map/ppermute | solution.py:27
  132.8 45.7 %collective-permute-start.21 = (bf16[352,2048]{1,0:T(8,128)(2,1)S(1)}, bf16[352,2048]{1,0:T(8,128)(2,1)S(1)}, u32[]{:S(2)}, u32[]{:S(2)}) collective-permute-start(bf16[352,2048]{1,0:T(8,128)(2,1)S(1)} %broadcast_select_fusion), channel_id=1, source_target_pairs={{0,1},{1,2},{2,3},{3,0},{4,7},{5,4},{6,5},{7,6},{8,9},{9,10},{10,1... | collective-permute-start | bytes 4325384 | tf_op jit(solution)/shard_map/ppermute | solution.py:51
  165.1 9.1 %collective-permute-start.15 = (bf16[3,800,128]{2,1,0:T(8,128)(2,1)S(1)}, bf16[3,800,128]{2,1,0:T(8,128)(2,1)S(1)}, u32[]{:S(2)}, u32[]{:S(2)}) collective-permute-start(bf16[3,800,128]{2,1,0:T(8,128)(2,1)S(1)} %get-tuple-element.31), channel_id=1, source_target_pairs={{0,4},{4,0},{1,5},{5,1},{2,6},{6,2},{3,7},{7,3},{8,12},{12,8},{9,1... | collective-permute-start | bytes 1843208 | tf_op jit(solution)/shard_map/ppermute | solution.py:27
  173.6 7.8 %collective-permute-start.14 = (bf16[800,128]{1,0:T(8,128)(2,1)S(1)}, bf16[800,128]{1,0:T(8,128)(2,1)S(1)}, u32[]{:S(2)}, u32[]{:S(2)}) collective-permute-start(bf16[800,128]{1,0:T(8,128)(2,1)S(1)} %get-tuple-element.29), channel_id=1, source_target_pairs={{0,4},{4,0},{1,5},{5,1},{2,6},{6,2},{3,7},{7,3},{8,12},{12,8},{9,1... | collective-permute-start | bytes 614408 | tf_op jit(solution)/shard_map/ppermute | solution.py:27
  174.9 8.0 %collective-permute-start.16 = (bf16[800,128]{1,0:T(8,128)(2,1)S(1)}, bf16[800,128]{1,0:T(8,128)(2,1)S(1)}, u32[]{:S(2)}, u32[]{:S(2)}) collective-permute-start(bf16[800,128]{1,0:T(8,128)(2,1)S(1)} %get-tuple-element.32), channel_id=1, source_target_pairs={{0,24},{8,0},{16,8},{24,16},{1,25},{9,1},{17,9},{25,17},{2,26},{10... | collective-permute-start | bytes 614408 | tf_op jit(solution)/shard_map/ppermute | solution.py:27
  175.4 7.6 %collective-permute-start.17 = (bf16[800,128]{1,0:T(8,128)(2,1)S(1)}, bf16[800,128]{1,0:T(8,128)(2,1)S(1)}, u32[]{:S(2)}, u32[]{:S(2)}) collective-permute-start(bf16[800,128]{1,0:T(8,128)(2,1)S(1)} %get-tuple-element.33), channel_id=1, source_target_pairs={{0,8},{8,16},{16,24},{24,0},{1,9},{9,17},{17,25},{25,1},{2,10},{10... | collective-permute-start | bytes 614408 | tf_op jit(solution)/shard_map/ppermute | solution.py:27
  177.0 10.2 %collective-permute-start.18 = (bf16[800,128]{1,0:T(8,128)(2,1)S(1)}, bf16[800,128]{1,0:T(8,128)(2,1)S(1)}, u32[]{:S(2)}, u32[]{:S(2)}) collective-permute-start(bf16[800,128]{1,0:T(8,128)(2,1)S(1)} %get-tuple-element.34), channel_id=1, source_target_pairs={{0,16},{8,24},{16,0},{24,8},{1,17},{9,25},{17,1},{25,9},{2,18},{10... | collective-permute-start | bytes 614408 | tf_op jit(solution)/shard_map/ppermute | solution.py:27
  188.6 7.1 %collective-permute-start.22 = (bf16[192,128]{1,0:T(8,128)(2,1)}, bf16[192,128]{1,0:T(8,128)(2,1)S(1)}, u32[]{:S(2)}, u32[]{:S(2)}) collective-permute-start(bf16[192,128]{1,0:T(8,128)(2,1)} %get-tuple-element.38), channel_id=1, source_target_pairs={{0,3},{1,0},{2,1},{3,2},{4,7},{5,4},{6,5},{7,6},{8,11},{9,8},{10,9... | collective-permute-start | bytes 147464 | tf_op jit(solution)/shard_map/ppermute | solution.py:27
  (25 other events, 117.5 us)
